TPU v7x, 128 devices: a whole 4x4x4 slice. The times are simulated.
128 devices in a mesh: sp: 32 (over z, y, core), tp: 4 (over x).
Axes of the slice: x: 4, y: 4, z: 4, core: 2. Of those that a mesh axis runs over, the one named last changes fastest.
Arguments:
- tokens: bfloat16 [32768, 2048], P('sp', 'tp'), may hold values from -6 to 6
- mix_gain: float32 [2048], replicated, may hold values from 0.1 to 1.9
- query_weight: bfloat16 [2048, 1024], P('sp', 'tp'), may hold values from -0.125 to 0.125
- key_weight: bfloat16 [2048, 256], P('sp', 'tp'), may hold values from -0.125 to 0.125
- value_weight: bfloat16 [2048, 256], P('sp', 'tp'), may hold values from -0.125 to 0.125
- conv_value_weight: bfloat16 [2048, 1024], P('sp', 'tp'), may hold values from -0.125 to 0.125
- conv_gate_weight: bfloat16 [2048, 1024], P('sp', 'tp'), may hold values from -0.125 to 0.125
- query_gain: float32 [64], replicated, may hold values from 0.1 to 1.9
- key_gain: float32 [64], replicated, may hold values from 0.1 to 1.9
- sink_logit: float32 [16], P('tp'), may hold values from 3 to 7
- conv_taps: float32 [31, 1024], P(None, 'tp'), may hold values from -1 to 1
- conv_gain: float32 [1024], P('tp'), may hold values from 0.1 to 1.9
- attn_proj: bfloat16 [1024, 2048], P('tp', 'sp'), may hold values from -1.5 to 1.5
- conv_proj: bfloat16 [1024, 2048], P('tp', 'sp'), may hold values from -0.1875 to 0.1875
Outputs:
- mixed: bfloat16 [32768, 2048], P(('sp', 'tp'))
All inputs are finite; a program needn't handle non-finite values.
Results may differ from a plain program's by a relative error of at most 0.0079.
Values may be sent and summed in bfloat16 or wider, within the bound.
A program may use at most 128 MiB of HBM per device.

v0:
```python
import jax
import jax.numpy as jnp
from jax import lax
from jax.sharding import PartitionSpec as P

WINDOW = 128


EPSILON = 0.1


def copy_for_each(value, axis):
    length = lax.axis_size(axis)
    return lax.all_to_all(
        jnp.broadcast_to(value[None], (length, *value.shape)), axis, 0, 0, tiled=True
    )


def laid_out(pieces, dim):
    pieces = jnp.moveaxis(pieces, 0, dim)
    lengths = pieces.shape
    return pieces.reshape(*lengths[:dim], lengths[dim] * lengths[dim + 1], *lengths[dim + 2 :])


def gather_directly(value, axis, dim):
    pieces = copy_for_each(value, axis)
    return laid_out(pieces, dim)


def side_by_side(arrays, axis, dim, along):
    ends, at = ([], 0)
    for a in arrays[:-1]:
        at += a.shape[along]
        ends.append(at)
    both = jnp.concatenate(arrays, axis=along)
    return tuple(jnp.split(lax.all_gather(both, axis, axis=dim, tiled=True), ends, axis=along))


def padded(value, sides, width):
    for axis, dim in sides:
        size, length = (lax.axis_size(axis), value.shape[dim])
        up = [(i, (i + 1) % size) for i in range(size - 1)]
        down = [(j, i) for i, j in up]
        last = lax.slice_in_dim(value, length - width, length, axis=dim)
        leading = lax.slice_in_dim(value, 0, width, axis=dim)
        before = lax.ppermute(last, axis, up)
        after = lax.ppermute(leading, axis, down)
        value = jnp.concatenate([before, value, after], axis=dim)
    return value


def rows_first(arrays, axis, dims):
    turned = [jnp.moveaxis(a, dim, 0) for a, dim in zip(arrays, dims)]
    widths = [t[0].size for t in turned]
    both = jnp.concatenate([t.reshape(-1, w) for t, w in zip(turned, widths)], axis=1)
    filled = lax.all_gather(both, axis, axis=0, tiled=True)
    pieces = jnp.split(filled, [sum(widths[:k]) for k in range(1, len(widths))], axis=1)
    return tuple(
        (
            jnp.moveaxis(b.reshape(-1, *t.shape[1:]), 0, dim)
            for b, t, dim in zip(pieces, turned, dims)
        )
    )


def unit_rows(values, gain):
    return values * lax.rsqrt(jnp.mean(values * values, axis=-1, keepdims=True) + EPSILON) * gain


def attend(queries, keys, values, sinks, offset, total):
    scale = queries.shape[-1] ** (-0.5)
    scores = jnp.einsum("qkgd,skd->kgqs", queries, keys, preferred_element_type=jnp.float32) * scale
    query_pos = offset + jnp.arange(queries.shape[0], dtype=jnp.int32)
    key_pos = offset - WINDOW + jnp.arange(keys.shape[0], dtype=jnp.int32)
    allowed = (
        (jnp.abs(key_pos[None, :] - query_pos[:, None]) <= WINDOW)
        & (key_pos[None, :] >= 0)
        & (key_pos[None, :] < total)
    )
    weights = jnp.where(allowed, jnp.exp(scores), 0.0)
    denominator = jnp.sum(weights, axis=-1, keepdims=True) + jnp.exp(sinks).reshape(
        keys.shape[1], -1, 1, 1
    )
    shares = (weights / denominator).astype(jnp.bfloat16)
    result = jnp.einsum("kgqs,skd->qkgd", shares, values, preferred_element_type=jnp.float32)
    return result.reshape(queries.shape[0], -1).astype(jnp.bfloat16)


def depthwise(extended, kernel_taps, count):
    result = jnp.zeros((count, kernel_taps.shape[1]), jnp.float32)
    for offset in range(kernel_taps.shape[0]):
        result = result + kernel_taps[offset] * extended[offset : offset + count]
    return result


def on_device(
    tokens,
    mix_gain,
    query_weight,
    key_weight,
    value_weight,
    conv_value_weight,
    conv_gate_weight,
    query_gain,
    key_gain,
    sink_logit,
    conv_taps,
    conv_gain,
    attn_proj,
    conv_proj,
):
    count = tokens.shape[0]
    whole = gather_directly(tokens, "tp", 1)
    normed = unit_rows(whole.astype(jnp.float32), mix_gain).astype(jnp.bfloat16)
    pieces = side_by_side(
        (query_weight, key_weight, value_weight, conv_value_weight, conv_gate_weight), "sp", 0, 1
    )
    query, key_part, value_part, conv_value, conv_gate = tuple(
        (jnp.dot(normed, piece, preferred_element_type=jnp.float32) for piece in pieces)
    )
    head_size = query_gain.shape[0]
    local_kv = key_part.shape[1] // head_size
    group = query.shape[1] // head_size // local_kv
    queries = unit_rows(query.reshape(count, local_kv, group, head_size), query_gain).astype(
        jnp.bfloat16
    )
    keys_normed = (
        unit_rows(key_part.reshape(count, local_kv, head_size), key_gain)
        .astype(jnp.bfloat16)
        .reshape(count, -1)
    )
    values_cast = value_part.astype(jnp.bfloat16)
    gated = (conv_value * jax.nn.sigmoid(conv_gate)).astype(jnp.bfloat16)
    reach = (conv_taps.shape[0] - 1) // 2
    kv_width = keys_normed.shape[1]
    joined = jnp.concatenate([keys_normed, values_cast, gated], axis=1)
    extended = padded(joined, (("sp", 0),), WINDOW)
    key_rows = extended[:, :kv_width]
    value_rows = extended[:, kv_width : 2 * kv_width]
    conv_rows = extended[WINDOW - reach : WINDOW + count + reach, 2 * kv_width :]
    offset = lax.axis_index("sp") * count
    total = count * lax.axis_size("sp")
    span_rows = key_rows.shape[0]
    attended = attend(
        queries,
        key_rows.reshape(span_rows, local_kv, head_size),
        value_rows.reshape(span_rows, local_kv, head_size),
        sink_logit,
        offset,
        total,
    )
    convolved = depthwise(conv_rows, conv_taps, count)
    all_channels = conv_taps.shape[1] * lax.axis_size("tp")
    sums, squares = lax.psum(
        (jnp.sum(convolved, axis=1), jnp.sum(convolved * convolved, axis=1)), "tp"
    )
    center = sums / all_channels
    spread = squares / all_channels - center * center
    centered = convolved - center[:, None]
    featured = jax.nn.silu(centered * lax.rsqrt(spread[:, None] + EPSILON) * conv_gain).astype(
        jnp.bfloat16
    )
    attn_full, conv_full = rows_first((attn_proj, conv_proj), "sp", (1, 1))
    summed = lax.psum_scatter(
        jnp.dot(attended, attn_full, preferred_element_type=jnp.float32)
        + jnp.dot(featured, conv_full, preferred_element_type=jnp.float32),
        "tp",
        scatter_dimension=0,
        tiled=True,
    )
    return summed.astype(jnp.bfloat16)


def solution(mesh):
    placed = (
        P("sp", "tp"),
        P(),
        P("sp", "tp"),
        P("sp", "tp"),
        P("sp", "tp"),
        P("sp", "tp"),
        P("sp", "tp"),
        P(),
        P(),
        P("tp"),
        P(None, "tp"),
        P("tp"),
        P("tp", "sp"),
        P("tp", "sp"),
    )
    return jax.shard_map(
        on_device, mesh=mesh, in_specs=placed, out_specs=P(("sp", "tp"), None), check_vma=False
    )
```

profile of v0, /device:TPU:1, one launch (start us, length us, event | category | flops | bytes accessed | tf_op | source)
XLA Modules:
  0.0 227.4 jit_solution(3349678265038607364)
XLA Ops:
  6.5 0.0 all-gather.3.cloned.1.call-start
  6.5 1.6 concatenate.46
  8.1 0.0 all-gather.3.cloned.1.call-update
  8.1 1.5 copy.16
  9.6 2.5 %broadcast_in_dim.8 = bf16[4,1024,512]{1,2,0:T(8,128)(2,1)} broadcast(bf16[1024,512]{0,1:T(8,128)(2,1)S(1)} %copy.16), dimensions={1,2} | broadcast | bytes 5242880 | tf_op jit(solution)/shard_map/broadcast_in_dim | solution.py:15
  12.1 0.0 copy-start.5
  12.1 5.0 %all-to-all-start = ((bf16[4,1024,512]{1,2,0:T(8,128)(2,1)}), bf16[4,1024,512]{1,2,0:T(8,128)(2,1)}, u32[]{:S(2)}, u32[]{:S(2)}) async-start(bf16[4,1024,512]{1,2,0:T(8,128)(2,1)} %broadcast_in_dim.8), calls=%async_computation | async-start | bytes 8388608 | tf_op jit(solution)/shard_map/all_to_all | solution.py:14
  17.1 0.0 copy-start.6
  17.1 0.0 all-gather.5.cloned.1.call-start
  17.2 0.0 copy-done.3
  17.2 0.0 copy-done.4
  17.2 0.6 pad_maximum_fusion.11
  17.8 0.0 all-gather.5.cloned.1.call-update
  17.9 0.0 reduce-scatter.2.cloned.1.call-start
  18.0 0.1 mul.455
  18.2 2.3 fusion.5
  20.4 45.5 %all-to-all-done = bf16[4,1024,512]{1,2,0:T(8,128)(2,1)} async-done(((bf16[4,1024,512]{1,2,0:T(8,128)(2,1)}), bf16[4,1024,512]{1,2,0:T(8,128)(2,1)}, u32[]{:S(2)}, u32[]{:S(2)}) %all-to-all-start) | async-done | bytes 4194336 | tf_op jit(solution)/shard_map/all_to_all | solution.py:14
  65.9 3.1 %multiply_reduce_fusion = f32[1024]{0:T(1024)S(1)} fusion(bf16[4,1024,512]{1,2,0:T(8,128)(2,1)} %all-to-all-done), kind=kLoop, calls=%fused_computation.7 | loop fusion | flops 6290432 | bytes 4198400 | tf_op jit(solution)/shard_map/reduce_sum | solution.py:67
  69.1 0.0 copy-done.6
  69.1 4.1 %fusion.3 = bf16[1024,2048]{0,1:T(8,128)(2,1)} fusion(f32[2048]{0:T(1024)S(1)} %copy-done.6, f32[1024]{0:T(1024)S(1)} %add_rsqrt_fusion.3, bf16[4,1024,512]{1,2,0:T(8,128)(2,1)} %all-to-all-done), kind=kLoop, calls=%fused_computation.6 | loop fusion | flops 8388608 | bytes 8400896 | tf_op jit(solution)/shard_map/convert_element_type | solution.py:114
  73.2 3.4 %multiply_reduce_fusion.2 = (f32[1024]{0:T(1024)S(1)}, f32[1024,64]{0,1:T(8,128)S(1)}) fusion(bf16[1024,2048]{0,1:T(8,128)(2,1)} %fusion.3, bf16[2048,896]{1,0:T(8,128)(2,1)} %all-gather.3.cloned.1.call-done), kind=kOutput, calls=%fused_computation.44 | convolution fusion | flops 268565504 | bytes 4984832 | tf_op jit(solution)/shard_map/dot_general | solution.py:119
  76.6 0.0 copy-done.8
  76.6 0.1 multiply_convert_fusion.2
  76.7 0.2 copy-done
  76.9 2.9 %fusion.8 = f32[1024,256]{0,1:T(8,128)S(1)} fusion(bf16[1024,2048]{0,1:T(8,128)(2,1)S(1)} %copy-done, bf16[2048,896]{1,0:T(8,128)(2,1)} %all-gather.3.cloned.1.call-done), kind=kOutput, calls=%fused_computation.16 | convolution fusion | flops 1074528256 | bytes 6291456 | tf_op jit(solution)/shard_map/dot_general | solution.py:119
  79.7 1.1 convolution_convert_fusion
  80.8 1.3 fusion.9
  82.2 3.5 %collective-permute-start.1 = (bf16[128,384]{0,1:T(8,128)(2,1)S(1)}, bf16[128,384]{0,1:T(8,128)(2,1)S(1)}, u32[]{:S(2)}, u32[]{:S(2)}) collective-permute-start(bf16[128,384]{0,1:T(8,128)(2,1)S(1)} %get-tuple-element.13), channel_id=1, source_target_pairs={{4,0},{8,4},{12,8},{16,12},{20,16},{24,20},{28,24},{32,28},{36,32}... | collective-permute-start | bytes 294920 | tf_op jit(solution)/shard_map/ppermute | solution.py:47
  85.7 3.3 %collective-permute-start = (bf16[128,384]{0,1:T(8,128)(2,1)S(1)}, bf16[128,384]{0,1:T(8,128)(2,1)S(1)}, u32[]{:S(2)}, u32[]{:S(2)}) collective-permute-start(bf16[128,384]{0,1:T(8,128)(2,1)S(1)} %get-tuple-element.12), channel_id=1, source_target_pairs={{0,4},{4,8},{8,12},{12,16},{16,20},{20,24},{24,28},{28,32},{32,36}... | collective-permute-start | bytes 294920 | tf_op jit(solution)/shard_map/ppermute | solution.py:46
  89.0 1.3 bitcast_reduce_fusion
  90.4 0.9 fusion.21
  91.3 0.0 collective-permute-done.1
  91.3 0.6 collective-permute-done
  91.9 0.2 maximum_maximum_fusion
  92.1 7.0 %fusion.45 = (f32[1024]{0:T(1024)S(1)}, f32[1024]{0:T(1024)S(1)}, f32[1024,256]{0,1:T(8,128)S(1)}) fusion(bf16[1152,384]{0,1:T(8,128)(2,1)S(1)} %get-tuple-element.11, f32[256]{0:T(256)S(1)} %bitcast.93, f32[256]{0:T(256)S(1)} %bitcast.94, f32[256]{0:T(256)S(1)} %bitcast.96, f32[256]{0:T(256)S(1)} %bitcast.97, f32[256]{0:T(256)S(1)} %bitcast.98, ...), kind=kLoop, calls=%fused_computation.77 | loop fusion | flops 24901632 | bytes 17341440 | tf_op jit(solution)/shard_map/reduce_sum | solution.py:155
  99.1 7.3 %all-reduce = (f32[1024]{0:T(1024)S(1)}, f32[1024]{0:T(1024)S(1)}) all-reduce(f32[1024]{0:T(1024)S(1)} %get-tuple-element.6, f32[1024]{0:T(1024)S(1)} %get-tuple-element.5), channel_id=1, replica_groups=mesh['sp'=32,'tp'=4] {'tp'}, use_global_device_ids=true, to_apply=%region_7.8 | all-reduce | flops 2048 | bytes 16384 | tf_op jit(solution)/shard_map/psum | solution.py:154
  106.4 11.0 %fusion.48 = (f32[4,1024]{1,0:T(4,128)S(1)}, f32[1,4,1024,1280]{2,3,1,0:T(8,128)}) fusion(bf16[1024,4,64]{0,2,1:T(8,128)(2,1)} %bitcast.80, bf16[128,384]{0,1:T(8,128)(2,1)S(1)} %collective-permute-done.1, bf16[128,384]{0,1:T(8,128)(2,1)S(1)} %collective-permute-done, bf16[1024,256]{0,1:T(8,128)(2,1)S(1)} %fusion.9, ...), kind=kOutput, calls=%fused_computation.80 | convolution fusion | flops 687632384 | bytes 23805952 | tf_op jit(solution)/shard_map/qkgd,skd->kgqs/dot_general | solution.py:72
  117.4 0.1 broadcast_add_fusion
  117.5 8.9 %fusion.10 = bf16[64,4,1024]{2,0,1:T(8,128)(2,1)S(1)} fusion(f32[1,4,1024,1280]{2,3,1,0:T(8,128)} %get-tuple-element.52, f32[4,1024]{1,0:T(4,128)S(1)} %broadcast_add_fusion, bf16[128,384]{0,1:T(8,128)(2,1)S(1)} %collective-permute-done.1, bf16[128,384]{0,1:T(8,128)(2,1)S(1)} %collective-permute-done, bf16[1024,256]{0,1:T(8,128)(2,1)S(1)} %fusion.9, ...), kind=kOutput, calls=%fused_computation.18 | convolution fusion | flops 682655744 | bytes 22495232 | tf_op jit(solution)/shard_map/kgqs,skd->qkgd/dot_general | solution.py:85
  126.4 0.0 all-gather.5.cloned.1.call-done
  126.4 0.0 copy-start.7
  126.4 2.7 %fusion.14 = f32[1024,2048]{1,0:T(8,128)S(1)} fusion(bf16[1024,256]{0,1:T(8,128)(2,1)S(1)} %bitcast.79, bf16[2048,512]{1,0:T(8,128)(2,1)} %all-gather.5.cloned.1.call-done), kind=kOutput, calls=%fused_computation.21 | convolution fusion | flops 1073741824 | bytes 9961472 | tf_op jit(solution)/shard_map/dot_general | solution.py:165
  129.1 0.0 copy-done.1
  129.1 0.0 copy-done.7
  129.1 4.8 %convolution_add_fusion = f32[1024,2048]{1,0:T(8,128)} fusion(f32[1024,2048]{1,0:T(8,128)S(1)} %fusion.14, bf16[2048,512]{1,0:T(8,128)(2,1)S(1)} %copy-done.1, f32[1024,256]{0,1:T(8,128)S(1)} %get-tuple-element.9, f32[256]{0:T(256)S(1)} %copy-done.7, f32[1024]{0:T(1024)S(1)} %get-tuple-element.46, f32[1024]{0:T(1024)S(1)} %get-tuple-element.45), kind=kOutput, calls=%fused_computation.11 | convolution fusion | flops 1077936128 | bytes 18883584 | tf_op jit(solution)/shard_map/dot_general | solution.py:166
  134.0 0.0 reduce-scatter.2.cloned.1.call-update
  134.0 84.2 %reduce-scatter.2.cloned.1.call-done = f32[256,2048]{1,0:T(8,128)} async-done(((f32[1024,2048]{1,0:T(8,128)}), f32[256,2048]{1,0:T(8,128)}) %reduce-scatter.2.cloned.1.call-update) | async-done | bytes 2097168 | tf_op jit(solution)/shard_map/reduce_scatter | solution.py:164
  218.1 2.7 %convert_element_type.196 = bf16[256,2048]{1,0:T(8,128)(2,1)} convert(f32[256,2048]{1,0:T(8,128)} %reduce-scatter.2.cloned.1.call-done) | non-fusion elementwise | flops 524288 | bytes 3145728 | tf_op jit(solution)/shard_map/convert_element_type | solution.py:171
  (25 shorter events, 0.1 us)
Async XLA Ops:
  6.5 66.7 %all-gather.3.cloned.1.call-start = ((), (), s32[]{:S(2)}) async-start(), calls=%async_computation.2 | async-start | bytes 3784704 | tf_op jit(solution)/shard_map/all_gather | solution.py:36
  12.1 5.1 %copy-start.3 = (bf16[256,64]{0,1:T(8,128)(2,1)S(1)}, bf16[256,64]{0,1:T(8,128)(2,1)}, u32[]{:S(2)}) copy-start(bf16[256,64]{0,1:T(8,128)(2,1)} %param.27) | copy-start | bytes 98308
  12.1 5.1 %copy-start.4 = (bf16[256,64]{0,1:T(8,128)(2,1)S(1)}, bf16[256,64]{0,1:T(8,128)(2,1)}, u32[]{:S(2)}) copy-start(bf16[256,64]{0,1:T(8,128)(2,1)} %param.26) | copy-start | bytes 98308
  12.1 5.8 %copy-start.9 = (f32[64]{0:T(128)S(1)}, f32[64]{0:T(128)}, u32[]{:S(2)}) copy-start(f32[64]{0:T(128)} %param.21) | copy-start | bytes 772
  12.1 5.9 %copy-start.10 = (f32[4]{0:T(128)S(1)}, f32[4]{0:T(128)}, u32[]{:S(2)}) copy-start(f32[4]{0:T(128)} %param.23) | copy-start | bytes 52
  12.1 6.0 %copy-start.5 = (f32[31,256]{1,0:T(8,128)S(1)}, f32[31,256]{1,0:T(8,128)}, u32[]{:S(2)}) copy-start(f32[31,256]{1,0:T(8,128)} %param.24) | copy-start | bytes 95236
  12.1 53.8 %all-to-all-start = ((bf16[4,1024,512]{1,2,0:T(8,128)(2,1)}), bf16[4,1024,512]{1,2,0:T(8,128)(2,1)}, u32[]{:S(2)}, u32[]{:S(2)}) async-start(bf16[4,1024,512]{1,2,0:T(8,128)(2,1)} %broadcast_in_dim.8), calls=%async_computation | async-start | bytes 8388608 | tf_op jit(solution)/shard_map/all_to_all | solution.py:14
  17.1 51.9 %copy-start.6 = (f32[2048]{0:T(1024)S(1)}, f32[2048]{0:T(1024)}, u32[]{:S(2)}) copy-start(f32[2048]{0:T(1024)} %param.15) | copy-start | bytes 24580
  17.1 109.3 %all-gather.5.cloned.1.call-start = ((), (), s32[]{:S(2)}) async-start(), calls=%async_computation.3 | async-start | bytes 2162688 | tf_op jit(solution)/shard_map/all_gather | solution.py:56
  17.9 200.2 %reduce-scatter.2.cloned.1.call-start = ((), (), s32[]{:S(2)}) async-start(), calls=%async_computation.4 | async-start | bytes 10485760 | tf_op jit(solution)/shard_map/reduce_scatter | solution.py:164
  73.2 3.4 %copy-start.8 = (f32[64]{0:T(128)S(1)}, f32[64]{0:T(128)}, u32[]{:S(2)}) copy-start(f32[64]{0:T(128)} %param.22) | copy-start | bytes 772
  73.2 3.7 %copy-start = (bf16[1024,2048]{0,1:T(8,128)(2,1)S(1)}, bf16[1024,2048]{0,1:T(8,128)(2,1)}, u32[]{:S(2)}) copy-start(bf16[1024,2048]{0,1:T(8,128)(2,1)} %fusion.3) | copy-start | bytes 12582916
  76.9 2.9 %copy-start.2 = (bf16[2048,896]{1,0:T(8,128)(2,1)S(1)}, bf16[2048,896]{1,0:T(8,128)(2,1)}, u32[]{:S(2)}) copy-start(bf16[2048,896]{1,0:T(8,128)(2,1)} %all-gather.3.cloned.1.call-done) | copy-start | bytes 11010052
  82.2 9.1 %collective-permute-start.1 = (bf16[128,384]{0,1:T(8,128)(2,1)S(1)}, bf16[128,384]{0,1:T(8,128)(2,1)S(1)}, u32[]{:S(2)}, u32[]{:S(2)}) collective-permute-start(bf16[128,384]{0,1:T(8,128)(2,1)S(1)} %get-tuple-element.13), channel_id=1, source_target_pairs={{4,0},{8,4},{12,8},{16,12},{20,16},{24,20},{28,24},{32,28},{36,32}... | collective-permute-start | bytes 294920 | tf_op jit(solution)/shard_map/ppermute | solution.py:47
  85.7 6.2 %collective-permute-start = (bf16[128,384]{0,1:T(8,128)(2,1)S(1)}, bf16[128,384]{0,1:T(8,128)(2,1)S(1)}, u32[]{:S(2)}, u32[]{:S(2)}) collective-permute-start(bf16[128,384]{0,1:T(8,128)(2,1)S(1)} %get-tuple-element.12), channel_id=1, source_target_pairs={{0,4},{4,8},{8,12},{12,16},{16,20},{20,24},{24,28},{28,32},{32,36}... | collective-permute-start | bytes 294920 | tf_op jit(solution)/shard_map/ppermute | solution.py:46
  126.4 2.7 %copy-start.1 = (bf16[2048,512]{1,0:T(8,128)(2,1)S(1)}, bf16[2048,512]{1,0:T(8,128)(2,1)}, u32[]{:S(2)}) copy-start(bf16[2048,512]{1,0:T(8,128)(2,1)} %all-gather.5.cloned.1.call-done) | copy-start | bytes 6291460
  126.4 2.7 %copy-start.7 = (f32[256]{0:T(256)S(1)}, f32[256]{0:T(256)}, u32[]{:S(2)}) copy-start(f32[256]{0:T(256)} %param.25) | copy-start | bytes 3076
Sparse Core Ops, SparseCore 0:
  9.6 49.2 all-gather.2
  61.1 43.2 all-gather.4
  134.1 83.9 reduce-scatter.1
where the time goes:
time: 228 us; the launch traced here: 227 us
  waiting for transfers between devices  130 us (57%)
  matrix products  37.3 us (16%)
  other arithmetic  21.2 us (9%)
  between operations  13.4 us (6%)
  starting transfers between devices  11.9 us (5%)
  blocking collectives  7.32 us (3%)
  local copies, waits for them, and re-layouts  5.9 us (3%)
    reduce_scatter x1, waiting for transfers between devices, on_device(): lax.psum_scatter(jnp.dot(attended, attn_full, preferred_element_type=jnp....  84.2 us
    all_to_all x1, waiting for transfers between devices, copy_for_each(): lax.all_to_all(jnp.broadcast_to(value[None], (length, *value.shape)), axi...  45.5 us
    dot_general x1, matrix products, attend(): jnp.einsum('qkgd,skd->kgqs', queries, keys, preferred_element_type=jnp.fl...  11 us
    dot_general x5, matrix products, on_device(): jnp.dot(normed, piece, preferred_element_type=jnp.float32)  9.92 us
    dot_general x1, matrix products, attend(): jnp.einsum('kgqs,skd->qkgd', shares, values, preferred_element_type=jnp.f...  8.9 us
    psum x1, blocking collectives, on_device(): lax.psum((jnp.sum(convolved, axis=1), jnp.sum(convolved * convolved, axis...  7.32 us
    reduce_sum x1, other arithmetic, on_device(): jnp.sum(convolved, axis=1)  7 us
    all_to_all x1, starting transfers between devices, copy_for_each(): lax.all_to_all(jnp.broadcast_to(value[None], (length, *value.shape)), axi...  4.98 us
  transfers between devices with their start and end apart: 6, of which 3 were waited for; matrix products, arithmetic and copies ran while one was open for 23% of the time, Pallas kernels for 0%

commit v1 on v0

v1 whole, which is shorter than its diff:
```python
import jax
import jax.numpy as jnp
from jax import lax
from jax.sharding import PartitionSpec as P

WINDOW = 128
EPSILON = 0.1
BOTH = ("sp", "tp")


def unit_rows(values, gain):
    return values * lax.rsqrt(jnp.mean(values * values, axis=-1, keepdims=True) + EPSILON) * gain


def halo(value, width):
    size = lax.axis_size("sp") * lax.axis_size("tp")
    up = [(i, i + 1) for i in range(size - 1)]
    down = [(i + 1, i) for i in range(size - 1)]
    before = lax.ppermute(value[-width:], BOTH, up)
    after = lax.ppermute(value[:width], BOTH, down)
    return jnp.concatenate([before, value, after], axis=0)


def attend(queries, keys, values, sinks, offset, total):
    scale = queries.shape[-1] ** (-0.5)
    scores = jnp.einsum("qkgd,skd->kgqs", queries, keys, preferred_element_type=jnp.float32) * scale
    query_pos = offset + jnp.arange(queries.shape[0], dtype=jnp.int32)
    key_pos = offset - WINDOW + jnp.arange(keys.shape[0], dtype=jnp.int32)
    allowed = (
        (jnp.abs(key_pos[None, :] - query_pos[:, None]) <= WINDOW)
        & (key_pos[None, :] >= 0)
        & (key_pos[None, :] < total)
    )
    weights = jnp.where(allowed, jnp.exp(scores), 0.0)
    denominator = jnp.sum(weights, axis=-1, keepdims=True) + jnp.exp(sinks).reshape(
        keys.shape[1], -1, 1, 1
    )
    shares = (weights / denominator).astype(jnp.bfloat16)
    result = jnp.einsum("kgqs,skd->qkgd", shares, values, preferred_element_type=jnp.float32)
    return result.reshape(queries.shape[0], -1).astype(jnp.bfloat16)


def depthwise(extended, kernel_taps, count):
    result = jnp.zeros((count, kernel_taps.shape[1]), jnp.float32)
    for offset in range(kernel_taps.shape[0]):
        result = result + kernel_taps[offset] * extended[offset : offset + count]
    return result


def on_device(tokens, mix_gain, wq, wk, wv, wcv, wcg, query_gain, key_gain, sinks, taps, conv_gain, attn_proj, conv_proj):
    tps = lax.axis_size("tp")
    count = tokens.shape[0] // tps
    w_in = lax.all_gather(jnp.concatenate([wq, wk, wv, wcv, wcg], axis=1), ("tp", "sp"), axis=0, tiled=True)
    w_in = w_in.reshape(tps, -1, w_in.shape[1])
    w_out = lax.all_gather(jnp.concatenate([attn_proj.T, conv_proj.T], axis=1), ("tp", "sp"), axis=0, tiled=True)
    w_out = w_out.reshape(tps, -1, w_out.shape[1])
    taps = jnp.moveaxis(lax.all_gather(taps, "tp"), 0, 1).reshape(taps.shape[0], -1)
    conv_gain = lax.all_gather(conv_gain, "tp", tiled=True)
    sinks = lax.all_gather(sinks, "tp", tiled=True)
    mine = lax.all_to_all(tokens.reshape(tps, count, -1), "tp", 0, 0, tiled=True)
    whole = jnp.moveaxis(mine, 0, 1).reshape(count, -1)
    normed = unit_rows(whole.astype(jnp.float32), mix_gain).astype(jnp.bfloat16)
    out = jnp.einsum("tk,pkc->tpc", normed, w_in, preferred_element_type=jnp.float32)
    head = query_gain.shape[0]
    widths = [wq.shape[1], wk.shape[1], wv.shape[1], wcv.shape[1]]
    ends = [sum(widths[: k + 1]) for k in range(4)]
    query, key_part, value_part, conv_value, conv_gate = jnp.split(out, ends, axis=2)
    kv = tps * key_part.shape[2] // head
    group = query.shape[2] * tps // head // kv
    queries = unit_rows(query.reshape(count, kv, group, head), query_gain).astype(jnp.bfloat16)
    keys = unit_rows(key_part.reshape(count, kv, head), key_gain).astype(jnp.bfloat16).reshape(count, -1)
    values = value_part.reshape(count, -1).astype(jnp.bfloat16)
    gated = (conv_value * jax.nn.sigmoid(conv_gate)).astype(jnp.bfloat16).reshape(count, -1)
    reach = (taps.shape[0] - 1) // 2
    ext_kv = halo(jnp.concatenate([keys, values], axis=1), WINDOW)
    ext_conv = halo(gated, 16)[16 - reach : 16 + count + reach]
    index = lax.axis_index("sp") * tps + lax.axis_index("tp")
    total = count * tps * lax.axis_size("sp")
    half = keys.shape[1]
    span = ext_kv.shape[0]
    attended = attend(
        queries, ext_kv[:, :half].reshape(span, kv, head), ext_kv[:, half:].reshape(span, kv, head),
        sinks, index * count, total,
    )
    convolved = depthwise(ext_conv, taps, count)
    center = jnp.mean(convolved, axis=1, keepdims=True)
    centered = convolved - center
    spread = jnp.mean(centered * centered, axis=1, keepdims=True)
    featured = jax.nn.silu(centered * lax.rsqrt(spread + EPSILON) * conv_gain).astype(jnp.bfloat16)
    feats = jnp.concatenate([attended.reshape(count, tps, -1), featured.reshape(count, tps, -1)], axis=2)
    mixed = jnp.einsum("tpk,pok->to", feats, w_out, preferred_element_type=jnp.float32)
    return mixed.astype(jnp.bfloat16)


def solution(mesh):
    placed = (
        P("sp", "tp"), P(), P("sp", "tp"), P("sp", "tp"), P("sp", "tp"), P("sp", "tp"), P("sp", "tp"),
        P(), P(), P("tp"), P(None, "tp"), P("tp"), P("tp", "sp"), P("tp", "sp"),
    )
    return jax.shard_map(
        on_device, mesh=mesh, in_specs=placed, out_specs=P(("sp", "tp"), None), check_vma=False
    )
```

time: 228 us -> 179 us (0.79)
  waiting for transfers between devices: 130 us -> 64.3 us
  blocking collectives: 7.32 us -> 29.6 us
  matrix products: 37.3 us -> 18.8 us
  starting transfers between devices: 11.9 us -> 17.3 us
  local copies, waits for them, and re-layouts: 5.9 us -> 11.1 us
    reduce_scatter x1 -> x0, waiting for transfers between devices: 84.2 us -> none  [on_device(): lax.psum_scatter(jnp.dot(attended, attn_full, preferred_element_type=jnp....]
    all_gather x2, waiting for transfers between devices: 0.02 us -> 60 us  [the longest x1 40.3 us: on_device(): lax.all_gather(jnp.concatenate([wq, wk, wv, wcv, wcg], axis=1), ('tp', 's...]
    all_to_all x1, waiting for transfers between devices: 45.5 us -> 0.01 us  [on_device(): lax.all_to_all(tokens.reshape(tps, count, -1), 'tp', 0, 0, tiled=True)]
    all_gather x0 -> x2, blocking collectives: none -> 16.9 us  [the longest x1 9.43 us: on_device(): lax.all_gather(taps, 'tp')]
    unnamed x0 -> x1, blocking collectives: none -> 12.7 us
    dot_general x1, matrix products: 11 us -> 2.75 us  [attend(): jnp.einsum('qkgd,skd->kgqs', queries, keys, preferred_element_type=jnp.fl...]
    reduce_sum x1 -> x2, other arithmetic: 7 us -> 14.7 us  [the longest x1 14.5 us: on_device(): center = jnp.mean(convolved, axis=1, keepdims=True)]
    psum x1 -> x0, blocking collectives: 7.32 us -> none  [on_device(): lax.psum((jnp.sum(convolved, axis=1), jnp.sum(convolved * convolved, axis...]
  transfers between devices with their start and end apart: 6 -> 7, of which waited for: 3 -> 3; matrix products, arithmetic and copies ran while one was open for 23% -> 24% of each run, Pallas kernels for 0% -> 0%
where the time goes in v1:
time: 179 us; the launch traced here: 178 us
  waiting for transfers between devices  64.3 us (36%)
  blocking collectives  29.6 us (17%)
  other arithmetic  22.6 us (13%)
  matrix products  18.8 us (11%)
  starting transfers between devices  17.3 us (10%)
  between operations  14.3 us (8%)
  local copies, waits for them, and re-layouts  11.1 us (6%)
    all_gather x1, waiting for transfers between devices, on_device(): lax.all_gather(jnp.concatenate([wq, wk, wv, wcv, wcg], axis=1), ('tp', 's...  40.3 us
    all_gather x1, waiting for transfers between devices, on_device(): lax.all_gather(jnp.concatenate([attn_proj.T, conv_proj.T], axis=1), ('tp'...  19.8 us
    reduce_sum x1, other arithmetic, on_device(): center = jnp.mean(convolved, axis=1, keepdims=True)  14.5 us
    unnamed x1, blocking collectives  12.7 us
    all_gather x1, blocking collectives, on_device(): lax.all_gather(taps, 'tp')  9.43 us
    all_gather x1, blocking collectives, on_device(): conv_gain = lax.all_gather(conv_gain, 'tp', tiled=True)  7.47 us
    dot_general x1, matrix products, on_device(): jnp.einsum('tk,pkc->tpc', normed, w_in, preferred_element_type=jnp.float32)  7.26 us
    ppermute x2, starting transfers between devices, halo(): after = lax.ppermute(value[:width], BOTH, down)  7.19 us
  transfers between devices with their start and end apart: 7, of which 3 were waited for; matrix products, arithmetic and copies ran while one was open for 24% of the time, Pallas kernels for 0%

profile of v1, /device:TPU:1, one launch (start us, length us, event | category | flops | bytes accessed | tf_op | source)
XLA Modules:
  0.0 178.1 jit_solution(16550307185612844283)
XLA Ops:
  6.5 1.6 concatenate.50
  8.2 1.4 pad_maximum_fusion.4
  9.6 4.8 %all-to-all-start = ((bf16[4,256,512]{2,1,0:T(8,128)(2,1)}), bf16[4,256,512]{2,1,0:T(8,128)(2,1)S(1)}, u32[]{:S(2)}, u32[]{:S(2)}) async-start(bf16[4,256,512]{2,1,0:T(8,128)(2,1)} %bitcast.91), calls=%async_computation | async-start | bytes 2097152 | tf_op jit(solution)/shard_map/all_to_all | solution.py:60
  14.4 0.7 mul.417
  15.1 1.3 dynamic-slice
  17.0 0.9 dynamic-update-slice
  17.9 12.7 %all-reduce = f32[16]{0:T(128)S(1)} all-reduce(f32[16]{0:T(128)S(1)} %dynamic-update-slice), channel_id=1, replica_groups=mesh['sp'=32,'tp'=4] {'tp'}, use_global_device_ids=true, to_apply=%add | all-reduce | flops 16 | bytes 128
  30.6 0.7 add.190
  31.3 7.5 %all-gather.2 = f32[4,1,256]{2,1,0:T(1,128)} all-gather(f32[1,1,256]{2,1,0:T(1,128)} %bitcast.134), channel_id=1, replica_groups=mesh['sp'=32,'tp'=4] {'tp'}, dimensions={0}, use_global_device_ids=true | all-gather | bytes 5120 | tf_op jit(solution)/shard_map/all_gather | solution.py:58
  38.7 9.4 %all-gather.1 = f32[4,31,256]{2,1,0:T(8,128)S(1)} all-gather(f32[1,31,256]{2,1,0:T(8,128)} %bitcast.98), channel_id=2, replica_groups=mesh['sp'=32,'tp'=4] {'tp'}, dimensions={0}, use_global_device_ids=true | all-gather | bytes 158720 | tf_op jit(solution)/shard_map/all_gather | solution.py:57
  48.2 0.6 fusion.59
  48.9 0.7 fusion.58
  49.5 0.3 fusion.48
  49.8 0.3 fusion.3
  50.1 0.3 fusion.7
  50.4 0.8 copy.31
  51.3 0.8 reshape.194
  52.1 40.3 %all-gather.6.cloned.1.call-done = bf16[8192,896]{1,0:T(8,128)(2,1)} async-done(((bf16[64,896]{1,0:T(8,128)(2,1)}), bf16[8192,896]{1,0:T(8,128)(2,1)}) %all-gather.6.cloned.1.call-update) | async-done | bytes 14680080 | tf_op jit(solution)/shard_map/all_gather | solution.py:53
  92.4 7.3 %fusion.60 = f32[256,4,896]{2,0,1:T(8,128)S(1)} fusion(bf16[256,2048,1]{1,0,2:T(8,128)(2,1)S(1)} %reshape.194, bf16[4,2048,896]{2,1,0:T(8,128)(2,1)} %bitcast.135), kind=kOutput, calls=%fused_computation.147 | convolution fusion | flops 3758096384 | bytes 19398656 | tf_op jit(solution)/shard_map/tk,pkc->tpc/dot_general | solution.py:63
  99.6 0.1 split.43
  99.8 0.2 multiply_reduce_fusion.2
  100.0 1.4 copy-done
  101.4 0.2 multiply_convert_fusion.3
  101.6 0.1 copy.32
  101.8 0.1 copy.33
  101.9 0.7 fusion.49
  102.6 3.1 %collective-permute-start = (bf16[128,512]{0,1:T(8,128)(2,1)}, bf16[128,512]{0,1:T(8,128)(2,1)}, u32[]{:S(2)}, u32[]{:S(2)}) collective-permute-start(bf16[128,512]{0,1:T(8,128)(2,1)} %get-tuple-element.13), channel_id=1, source_target_pairs={{0,1},{1,2},{2,3},{3,4},{4,5},{5,6},{6,7},{7,8},{8,9},{9,10},{10,1... | collective-permute-start | bytes 393224 | tf_op jit(solution)/shard_map/ppermute | solution.py:19
  105.7 3.7 %collective-permute-start.1 = (bf16[128,512]{0,1:T(8,128)(2,1)}, bf16[128,512]{0,1:T(8,128)(2,1)}, u32[]{:S(2)}, u32[]{:S(2)}) collective-permute-start(bf16[128,512]{0,1:T(8,128)(2,1)} %get-tuple-element.14), channel_id=1, source_target_pairs={{1,0},{2,1},{3,2},{4,3},{5,4},{6,5},{7,6},{8,7},{9,8},{10,9},{11,1... | collective-permute-start | bytes 393224 | tf_op jit(solution)/shard_map/ppermute | solution.py:20
  109.4 2.2 %fusion.56 = (f32[256,4,256]{2,0,1:T(8,128)S(1)}, bf16[256,4,256]{2,0,1:T(8,128)(2,1)S(1)}) fusion(f32[256,4,896]{2,0,1:T(8,128)} %copy-done), kind=kLoop, calls=%fused_computation.143 | loop fusion | flops 1310720 | bytes 4718592 | tf_op jit(solution)/shard_map/split | solution.py:67
  111.6 0.3 copy.34
  111.9 0.2 copy.46
  112.1 3.5 %collective-permute-start.3 = (bf16[16,1024]{0,1:T(8,128)(2,1)S(1)}, bf16[16,1024]{0,1:T(8,128)(2,1)S(1)}, u32[]{:S(2)}, u32[]{:S(2)}) collective-permute-start(bf16[16,1024]{0,1:T(8,128)(2,1)S(1)} %bitcast.95), channel_id=1, source_target_pairs={{1,0},{2,1},{3,2},{4,3},{5,4},{6,5},{7,6},{8,7},{9,8},{10,9},{11,1... | collective-permute-start | bytes 98312 | tf_op jit(solution)/shard_map/ppermute | solution.py:20
  115.6 2.1 %collective-permute-start.2 = (bf16[16,1024]{1,0:T(8,128)(2,1)S(1)}, bf16[16,1024]{1,0:T(8,128)(2,1)S(1)}, u32[]{:S(2)}, u32[]{:S(2)}) collective-permute-start(bf16[16,1024]{1,0:T(8,128)(2,1)S(1)} %bitcast.99), channel_id=1, source_target_pairs={{0,1},{1,2},{2,3},{3,4},{4,5},{5,6},{6,7},{7,8},{8,9},{9,10},{10,1... | collective-permute-start | bytes 98312 | tf_op jit(solution)/shard_map/ppermute | solution.py:19
  117.7 0.1 multiply_reduce_fusion.1
  117.9 0.2 copy.37
  118.1 4.2 %collective-permute-done.2 = bf16[16,1024]{1,0:T(8,128)(2,1)S(1)} collective-permute-done((bf16[16,1024]{1,0:T(8,128)(2,1)S(1)}, bf16[16,1024]{1,0:T(8,128)(2,1)S(1)}, u32[]{:S(2)}, u32[]{:S(2)}) %collective-permute-start.2) | collective-permute-done | bytes 32800 | tf_op jit(solution)/shard_map/ppermute | solution.py:19
  122.3 0.2 copy.38
  122.5 14.5 %fusion.55 = (f32[256]{0:T(256)S(1)}, f32[256,1024]{0,1:T(8,128)S(1)}) fusion(bf16[16,1024]{0,1:T(8,128)(2,1)S(1)} %collective-permute-done.3, bf16[256,1024]{0,1:T(8,128)(2,1)S(1)} %bitcast.86, f32[1024]{0:T(1024)} %bitcast.115, f32[1024]{0:T(1024)} %bitcast.116, f32[1024]{0:T(1024)} %bitcast.117, f32[1024]{0:T(1024)} %bitcast.118, f32[1024]{0:T(1024)} %bitcast.119, ...), kind=kLoop, calls=%fused_computation.142 | loop fusion | flops 47972096 | bytes 1766400 | tf_op jit(solution)/shard_map/reduce_sum | solution.py:86
  137.0 0.2 multiply_reduce_fusion
  137.2 1.1 multiply_convert_fusion
  138.3 0.2 copy.42
  138.5 1.0 pad_maximum_fusion.2
  139.6 2.8 %fusion = (f32[4,4,256]{2,1,0:T(4,128)S(1)}, f32[4,512,256,4]{2,1,3,0:T(8,128)S(1)}) fusion(pred[256,512]{0,1:T(8,128)(4,1)S(1)} %fusion.48, bf16[512,4,64,1]{0,2,3,1:T(8,128)(2,1)S(1)} %bitcast.97, f32[256,4,4,64]{0,3,2,1:T(8,128)S(1)} %bitcast.84, f32[64]{0:T(128)} %param.21, f32[256,4,4]{0,2,1:T(4,128)S(1)} %add_rsqrt_fusion), kind=kOutput, calls=%fused_computation.2 | convolution fusion | flops 275509248 | bytes 9863424 | tf_op jit(solution)/shard_map/qkgd,skd->kgqs/dot_general | solution.py:26
  142.4 0.1 broadcast_add_fusion
  142.4 2.1 %fusion.6 = bf16[4,64,4,256]{3,1,2,0:T(8,128)(2,1)S(1)} fusion(bf16[512,4,64,1]{0,2,3,1:T(8,128)(2,1)S(1)} %bitcast.96, f32[4,512,256,4]{2,1,3,0:T(8,128)S(1)} %get-tuple-element.47, f32[4,4,256]{2,1,0:T(4,128)S(1)} %broadcast_add_fusion, pred[256,512]{0,1:T(8,128)(4,1)S(1)} %fusion.48), kind=kOutput, calls=%fused_computation.39 | convolution fusion | flops 277086208 | bytes 9322496 | tf_op jit(solution)/shard_map/kgqs,skd->qkgd/dot_general | solution.py:39
  144.5 0.2 copy.41
  144.8 19.8 %all-gather.8.cloned.1.call-done = bf16[8192,512]{1,0:T(8,128)(2,1)} async-done(((bf16[64,512]{1,0:T(8,128)(2,1)}), bf16[8192,512]{1,0:T(8,128)(2,1)}) %all-gather.8.cloned.1.call-update) | async-done | bytes 8388624 | tf_op jit(solution)/shard_map/all_gather | solution.py:55
  164.5 6.7 %fusion.2 = bf16[256,2048]{1,0:T(8,128)(2,1)} fusion(bf16[4,2048,512]{2,1,0:T(8,128)(2,1)} %bitcast.136, bf16[256,4,256]{2,0,1:T(8,128)(2,1)S(1)} %copy.42, bf16[256,4,256]{2,0,1:T(8,128)(2,1)S(1)} %copy.41), kind=kOutput, calls=%fused_computation.35 | convolution fusion | flops 2150105088 | bytes 10485760 | tf_op jit(solution)/shard_map/tpk,pok->to/dot_general | solution.py:91
  (26 shorter events, 0.2 us)
Async XLA Ops:
  6.5 85.8 %all-gather.6.cloned.1.call-start = ((), (), s32[]{:S(2)}) async-start(), calls=%async_computation.1 | async-start | bytes 14794752 | tf_op jit(solution)/shard_map/all_gather | solution.py:53
  8.1 156.4 %all-gather.8.cloned.1.call-start = ((), (), s32[]{:S(2)}) async-start(), calls=%async_computation.2 | async-start | bytes 8454144 | tf_op jit(solution)/shard_map/all_gather | solution.py:55
  9.6 40.2 %all-to-all-start = ((bf16[4,256,512]{2,1,0:T(8,128)(2,1)}), bf16[4,256,512]{2,1,0:T(8,128)(2,1)S(1)}, u32[]{:S(2)}, u32[]{:S(2)}) async-start(bf16[4,256,512]{2,1,0:T(8,128)(2,1)} %bitcast.91), calls=%async_computation | async-start | bytes 2097152 | tf_op jit(solution)/shard_map/all_to_all | solution.py:60
  92.4 9.1 %copy-start.2 = (f32[64]{0:T(128)S(1)}, f32[64]{0:T(128)}, u32[]{:S(2)}) copy-start(f32[64]{0:T(128)} %param.22) | copy-start | bytes 772
  99.6 1.8 %copy-start = (f32[256,4,896]{2,0,1:T(8,128)}, f32[256,4,896]{2,0,1:T(8,128)S(1)}, u32[]{:S(2)}) copy-start(f32[256,4,896]{2,0,1:T(8,128)S(1)} %fusion.60) | copy-start | bytes 11010052
  102.6 35.9 %collective-permute-start = (bf16[128,512]{0,1:T(8,128)(2,1)}, bf16[128,512]{0,1:T(8,128)(2,1)}, u32[]{:S(2)}, u32[]{:S(2)}) collective-permute-start(bf16[128,512]{0,1:T(8,128)(2,1)} %get-tuple-element.13), channel_id=1, source_target_pairs={{0,1},{1,2},{2,3},{3,4},{4,5},{5,6},{6,7},{7,8},{8,9},{9,10},{10,1... | collective-permute-start | bytes 393224 | tf_op jit(solution)/shard_map/ppermute | solution.py:19
  105.7 32.8 %collective-permute-start.1 = (bf16[128,512]{0,1:T(8,128)(2,1)}, bf16[128,512]{0,1:T(8,128)(2,1)}, u32[]{:S(2)}, u32[]{:S(2)}) collective-permute-start(bf16[128,512]{0,1:T(8,128)(2,1)} %get-tuple-element.14), channel_id=1, source_target_pairs={{1,0},{2,1},{3,2},{4,3},{5,4},{6,5},{7,6},{8,7},{9,8},{10,9},{11,1... | collective-permute-start | bytes 393224 | tf_op jit(solution)/shard_map/ppermute | solution.py:20
  112.1 10.4 %collective-permute-start.3 = (bf16[16,1024]{0,1:T(8,128)(2,1)S(1)}, bf16[16,1024]{0,1:T(8,128)(2,1)S(1)}, u32[]{:S(2)}, u32[]{:S(2)}) collective-permute-start(bf16[16,1024]{0,1:T(8,128)(2,1)S(1)} %bitcast.95), channel_id=1, source_target_pairs={{1,0},{2,1},{3,2},{4,3},{5,4},{6,5},{7,6},{8,7},{9,8},{10,9},{11,1... | collective-permute-start | bytes 98312 | tf_op jit(solution)/shard_map/ppermute | solution.py:20
  115.6 6.7 %collective-permute-start.2 = (bf16[16,1024]{1,0:T(8,128)(2,1)S(1)}, bf16[16,1024]{1,0:T(8,128)(2,1)S(1)}, u32[]{:S(2)}, u32[]{:S(2)}) collective-permute-start(bf16[16,1024]{1,0:T(8,128)(2,1)S(1)} %bitcast.99), channel_id=1, source_target_pairs={{0,1},{1,2},{2,3},{3,4},{4,5},{5,6},{6,7},{7,8},{8,9},{9,10},{10,1... | collective-permute-start | bytes 98312 | tf_op jit(solution)/shard_map/ppermute | solution.py:19
  137.0 5.3 %copy-start.1 = (f32[4,4]{1,0:T(4,128)S(1)}, f32[4,4]{1,0:T(4,128)}, u32[]{:S(2)}) copy-start(f32[4,4]{1,0:T(4,128)} %add.190) | copy-start | bytes 196
Sparse Core Ops, SparseCore 0:
  10.2 82.1 all-gather.5
  95.3 69.1 all-gather.7

commit v2 on v1

v2 whole, which is shorter than its diff:
```python
import jax
import jax.numpy as jnp
from jax import lax
from jax.experimental import pallas as pl
from jax.experimental.pallas import tpu as pltpu
from jax.sharding import PartitionSpec as P

MESH = pl.DeviceIdType.MESH
EPSILON = 0.1
BF = jnp.bfloat16
F32 = jnp.float32

CV, CG, KV, Q = (0, 256), (256, 512), (512, 640), (640, 896)
STAGES = (
    ("w", 0, 640, ((0, 48, 32), (48, 32, 16), (80, 48, 32))),
    ("w", 640, 256, ((0, 32, 16), (32, 48, 32), (80, 48, 32))),
    ("p", 0, 128, ((0, 176, 96), (176, 160, 80), (336, 176, 96))),
)
ORDERS = ("xyz", "yzx", "zxy")


def kernel(
    tokens, mix_gain, wq, wk, wv, wcv, wcg, query_gain, key_gain, sink_row, taps, conv_gain, attn_proj, conv_proj,
    out,
    w, p, mine_w, mine_p, peer_p, small, x_buf, normed, qn, kve, ge, conv, stat_own, stat_peer, feats,
    part_own, part_send, part_recv,
    ag_send, ag_recv, d2d_send, d2d_recv, tok_send, tok_recv, fwd_send, fwd_recv, loc_sem, sm_send, sm_recv,
    halo_send, halo_recv, stat_send, stat_recv, out_send, out_recv,
):
    sp, x = lax.axis_index("sp"), lax.axis_index("tp")
    k = lax.rem(sp, 2)
    q = sp // 2
    y, z = lax.rem(q, 4), q // 4
    pos = lax.rem(x + 4 - 2 * k, 4)
    xi0 = lax.rem(x, 2)
    is_source = pos < 2
    bufs = {"w": w, "p": p}

    def dev(xx, yy, zz, kk):
        return (zz * 8 + yy * 2 + kk, xx)

    def up(v, n=1):
        return lax.rem(v + n, 4)

    peer = dev(x, y, z, 1 - k)
    sends = []

    def copy(src, dst, ssem, rsem, device):
        return pltpu.make_async_remote_copy(
            src_ref=src, dst_ref=dst, send_sem=ssem, recv_sem=rsem, device_id=device, device_id_type=MESH
        )

    def send(src, dst, ssem, rsem, device, cond=None):
        def go():
            copy(src, dst, ssem, rsem, device).start()

        if cond is None:
            go()
        else:
            pl.when(cond)(go)
        sends.append((src, dst, ssem, rsem, device, cond))

    def recv(dst, ssem, rsem, cond=None):
        def go():
            copy(dst, dst, ssem, rsem, peer).wait_recv()

        if cond is None:
            go()
        else:
            pl.when(cond)(go)

    def ref_of(stage, color, phase, where, half):
        name, c0, cn, rows = STAGES[stage]
        buf = bufs[name]
        r0, rn, rh = rows[color]
        cols = pl.ds(c0, cn)
        rr = pl.ds(r0, rn)
        parts = {None: rr, 0: pl.ds(r0, rh), 1: pl.ds(r0 + rh, rn - rh)}
        two = {None: slice(None), 0: pl.ds(0, 2), 1: pl.ds(2, 2)}
        one = {None: slice(None), 0: pl.ds(0, 1), 1: pl.ds(1, 1)}
        axis = ORDERS[color][phase]
        if phase == 0:
            if axis == "x":
                return buf.at[where, z, y, parts[half], cols]
            if axis == "y":
                return buf.at[xi0, z, where, parts[half], cols]
            return buf.at[xi0, where, y, parts[half], cols]
        if color == 0:
            if axis == "y":
                return buf.at[one[half], z, where, rr, cols]
            return buf.at[one[half], where, :, rr, cols]
        if color == 1:
            if axis == "z":
                return buf.at[xi0, where, two[half], rr, cols]
            return buf.at[where, two[half], :, rr, cols]
        if axis == "x":
            return buf.at[where, two[half], y, rr, cols]
        return buf.at[one[half], :, where, rr, cols]

    def context(stage, color, phase):
        axis = ORDERS[color][phase]
        base = ((stage * 3 + color) * 3 + phase) * 4
        ss = [ag_send.at[base + i] for i in range(4)]
        rs = [ag_recv.at[base + i] for i in range(4)]
        only_sources = is_source if ORDERS[color].index("x") > phase else None
        return axis, ss, rs, only_sources

    def ring(axis):
        if axis == "y":
            return y, dev(x, up(y), z, k), dev(x, up(y, 3), z, k)
        return z, dev(x, y, up(z), k), dev(x, y, up(z, 3), k)

    def start1(stage, color, phase):
        axis, ss, rs, cond = context(stage, color, phase)
        if axis == "x":
            r = ref_of(stage, color, phase, xi0, None)
            send(r, r, ss[0], rs[0], dev(up(x), y, z, k), is_source)
            send(r, r, ss[1], rs[0], dev(up(x, 3), y, z, k), is_source)
        else:
            at, right, left = ring(axis)
            r = ref_of(stage, color, phase, at, None)
            send(r, r, ss[0], rs[0], right, cond)
            send(r, r, ss[1], rs[1], left, cond)

    def turn(stage, color, phase):
        axis, ss, rs, cond = context(stage, color, phase)
        if axis == "x":
            other = 1 - xi0
            recv(ref_of(stage, color, phase, other, None), ss[0], rs[0])
            h0 = ref_of(stage, color, phase, other, 0)
            h1 = ref_of(stage, color, phase, other, 1)
            to_low = dev(jnp.where(pos == 0, up(x, 3), up(x)), y, z, k)
            to_high = dev(jnp.where(pos == 2, up(x), up(x, 3)), y, z, k)
            send(h0, h0, ss[2], rs[2], to_low, pos < 2)
            send(h1, h1, ss[3], rs[3], to_high, pos >= 2)
        else:
            at, right, left = ring(axis)
            recv(ref_of(stage, color, phase, up(at, 3), None), ss[0], rs[0], cond)
            h0 = ref_of(stage, color, phase, up(at, 3), 0)
            send(h0, h0, ss[2], rs[2], right, cond)
            recv(ref_of(stage, color, phase, up(at), None), ss[1], rs[1], cond)
            h1 = ref_of(stage, color, phase, up(at), 1)
            send(h1, h1, ss[3], rs[3], left, cond)

    def finish(stage, color, phase):
        axis, ss, rs, cond = context(stage, color, phase)
        if axis == "x":
            recv(ref_of(stage, color, phase, xi0, 0), ss[2], rs[2], pos >= 2)
            recv(ref_of(stage, color, phase, xi0, 1), ss[3], rs[3], pos >= 2)
        else:
            at, _, _ = ring(axis)
            recv(ref_of(stage, color, phase, up(at, 2), 0), ss[2], rs[2], cond)
            recv(ref_of(stage, color, phase, up(at, 2), 1), ss[3], rs[3], cond)

    def all_colors(step, stage, phase):
        for color in range(3):
            step(stage, color, phase)

    own_rows = pl.ds(pl.multiple_of(k * 64, 64), 64)
    shard = jnp.concatenate([wcv[...], wcg[...], wk[...], wv[...], wq[...]], axis=1)

    @pl.when(is_source)
    def _():
        w[xi0, z, y, own_rows, :] = shard

    @pl.when(jnp.logical_not(is_source))
    def _():
        mine_w[...] = shard

    mine_p[...] = jnp.concatenate([attn_proj[...], conv_proj[...]], axis=1)
    small[xi0, 0:31, :] = taps[...]
    small[xi0, 31:32, :] = conv_gain[...]
    small[xi0, 32:33, :] = sink_row[...]

    barrier = pltpu.get_barrier_semaphore()
    y_up, z_up = up(y), up(z)
    q_next, q_last = lax.rem(q + 1, 16), lax.rem(q + 15, 16)
    partners = [
        peer, dev(up(x), y, z, k), dev(up(x, 2), y, z, k), dev(up(x, 3), y, z, k),
        dev(x, y_up, z, k), dev(x, up(y, 3), z, k), dev(x, y, z_up, k), dev(x, y, up(z, 3), k),
        (q_next * 2 + k, up(x)), (q_last * 2 + k, up(x, 3)),
    ]
    for partner in partners:
        pl.semaphore_signal(barrier, inc=1, device_id=partner, device_id_type=MESH)
    pl.semaphore_wait(barrier, len(partners))

    not_source = jnp.logical_not(is_source)
    slot = w.at[xi0, z, y, own_rows, :]
    send(mine_w, slot, d2d_send.at[0], d2d_recv.at[0], peer, not_source)
    send(mine_p, peer_p, d2d_send.at[1], d2d_recv.at[1], peer)
    peer_rows = pl.ds(pl.multiple_of((1 - k) * 64, 64), 64)
    recv(w.at[xi0, z, y, peer_rows, :], d2d_send.at[0], d2d_recv.at[0], is_source)
    all_colors(start1, 0, 0)

    for d in (1, 3, 2):
        to = up(x, d)
        rows = pl.ds(pl.multiple_of(to * 256, 256), 256)
        send(tokens.at[rows, :], x_buf.at[k, x], tok_send.at[d], tok_recv.at[d], dev(to, y, z, k))
    rows = pl.ds(pl.multiple_of(x * 256, 256), 256)
    local = pltpu.make_async_copy(tokens.at[rows, :], x_buf.at[k, x], loc_sem)
    local.start()
    send(tokens.at[rows, :], x_buf.at[k, x], fwd_send.at[0], fwd_recv.at[0], peer)
    mine_small = small.at[xi0]
    for d in (1, 2, 3):
        send(mine_small, mine_small, sm_send.at[d], sm_recv.at[xi0], dev(up(x, d), y, z, k), is_source)

    all_colors(turn, 0, 0)
    all_colors(start1, 1, 0)
    all_colors(finish, 0, 0)
    all_colors(start1, 0, 1)

    recv(peer_p, d2d_send.at[1], d2d_recv.at[1])

    @pl.when(is_source)
    def _():
        a, b = mine_p[...], peer_p[...]
        low = jnp.where(k == 0, a, b)
        high = jnp.where(k == 0, b, a)
        p[xi0, z, y, 0:256, :] = jnp.concatenate([low[:, :64], high[:, :64]], axis=1)
        p[xi0, z, y, 256:512, :] = jnp.concatenate([low[:, 64:], high[:, 64:]], axis=1)

    all_colors(turn, 1, 0)
    all_colors(turn, 0, 1)
    all_colors(finish, 1, 0)
    all_colors(finish, 0, 1)
    all_colors(start1, 0, 2)
    all_colors(start1, 1, 1)
    all_colors(start1, 2, 0)

    for d in (1, 3, 2):
        origin = up(x, 4 - d)
        recv(x_buf.at[k, origin], tok_send.at[d], tok_recv.at[d])
        send(x_buf.at[k, origin], x_buf.at[k, origin], fwd_send.at[d], fwd_recv.at[d], peer)

    all_colors(turn, 2, 0)
    all_colors(turn, 1, 1)
    all_colors(finish, 2, 0)
    all_colors(finish, 1, 1)

    local.wait()
    recv(x_buf.at[1 - k, x], fwd_send.at[0], fwd_recv.at[0])
    for d in (1, 3, 2):
        recv(x_buf.at[1 - k, up(x, 4 - d)], fwd_send.at[d], fwd_recv.at[d])

    def norm_rows(i, _):
        s, r = i // 8, lax.rem(i, 8)
        rows = pl.ds(pl.multiple_of(r * 32, 32), 32)
        parts = [x_buf[s, f, rows, :].astype(F32) for f in range(4)]
        square = sum(jnp.sum(v * v, axis=-1, keepdims=True) for v in parts)
        scale = lax.rsqrt(square * (1.0 / 2048) + EPSILON)
        for f in range(4):
            normed[pl.ds(pl.multiple_of(i * 32, 32), 32), f * 512 : f * 512 + 512] = (
                parts[f] * scale * mix_gain[:, f * 512 : f * 512 + 512]
            ).astype(BF)
        return 0

    lax.fori_loop(0, 16, norm_rows, 0)

    all_colors(turn, 0, 2)
    all_colors(start1, 1, 2)
    all_colors(start1, 2, 1)
    all_colors(finish, 0, 2)

    lane = lax.broadcasted_iota(jnp.int32, (256, 128), 1)
    low_lane = lane < 64
    key_row = jnp.concatenate([key_gain[...], jnp.ones_like(key_gain[...])], axis=1)
    query_row = jnp.concatenate([query_gain[...], query_gain[...]], axis=1)

    def project(s, xi, cols):
        lhs = normed[pl.ds(pl.multiple_of(s * 256, 256), 256), :]
        rhs = w[xi, :, :, :, cols[0] : cols[1]].reshape(2048, cols[1] - cols[0])
        return jnp.dot(lhs, rhs, preferred_element_type=F32)

    def first_part(i, _):
        xi, s = i // 2, lax.rem(i, 2)
        kv = project(s, xi, KV)
        square = jnp.sum(jnp.where(low_lane, kv * kv, 0.0), axis=-1, keepdims=True)
        keyed = kv * lax.rsqrt(square * (1.0 / 64) + EPSILON) * key_row
        kve[s, xi, 128:384, :] = jnp.where(low_lane, keyed, kv).astype(BF)
        value, gate = project(s, xi, CV), project(s, xi, CG)
        gated = (value * jax.nn.sigmoid(gate)).astype(BF).astype(F32)
        ge[s, xi * 2, 16:272, :] = gated[:, :128]
        ge[s, xi * 2 + 1, 16:272, :] = gated[:, 128:]
        return 0

    lax.fori_loop(0, 4, first_part, 0)

    for s in (0, 1):
        for side in (0, 1):
            if side == 0:
                wraps = x == 3
                step = jnp.where(jnp.logical_and(wraps, s == 1), 1, 0)
                to = (lax.rem(q + step, 16) * 2 + k, up(x))
                src_kv, dst_kv, src_ge, dst_ge = (256, 0, 256, 0)
            else:
                wraps = x == 0
                step = jnp.where(jnp.logical_and(wraps, s == 0), 15, 0)
                to = (lax.rem(q + step, 16) * 2 + k, up(x, 3))
                src_kv, dst_kv, src_ge, dst_ge = (128, 384, 16, 272)
            seg = jnp.where(wraps, 1 - s, s)
            i = s * 4 + side * 2
            j = seg * 4 + side * 2
            send(kve.at[s, :, pl.ds(src_kv, 128), :], kve.at[seg, :, pl.ds(dst_kv, 128), :],
                 halo_send.at[i], halo_recv.at[j], to)
            send(ge.at[s, :, pl.ds(src_ge, 16), :], ge.at[seg, :, pl.ds(dst_ge, 16), :],
                 halo_send.at[i + 1], halo_recv.at[j + 1], to)

    all_colors(turn, 2, 1)
    all_colors(turn, 1, 2)
    all_colors(finish, 2, 1)
    all_colors(start1, 2, 2)

    for s in (0, 1):
        for side in (0, 1):
            i = s * 4 + side * 2
            recv(kve.at[s, :, pl.ds(0 if side == 0 else 384, 128), :], halo_send.at[i], halo_recv.at[i])
            recv(ge.at[s, :, pl.ds(0 if side == 0 else 272, 16), :], halo_send.at[i + 1], halo_recv.at[i + 1])
    is_first = jnp.logical_and(q == 0, x == 0)
    is_last = jnp.logical_and(q == 15, x == 3)

    @pl.when(is_first)
    def _():
        ge[0, :, 0:16, :] = jnp.zeros((4, 16, 128), F32)

    @pl.when(is_last)
    def _():
        ge[1, :, 272:288, :] = jnp.zeros((4, 16, 128), F32)

    recv(small.at[1 - xi0], sm_send.at[1], sm_recv.at[1 - xi0])
    recv(small.at[xi0], sm_send.at[1], sm_recv.at[xi0], not_source)

    def conv_block(i, _):
        s, cb = i // 4, lax.rem(i, 4)
        xi, half = cb // 2, lax.rem(cb, 2)
        tap_rows = jnp.where(half == 0, small[xi, :, 0:128], small[xi, :, 128:256])
        for r in (0, 128):
            total = jnp.zeros((128, 128), F32)
            for t in range(31):
                total = total + tap_rows[t : t + 1, :] * ge[s, cb, r + 1 + t : r + 129 + t, :]
            conv[cb, pl.ds(pl.multiple_of(s * 256, 256) + r, 128), :] = total
        return 0

    lax.fori_loop(0, 8, conv_block, 0)

    def stats(i, _):
        rows = pl.ds(pl.multiple_of(i * 64, 64), 64)
        blocks = [conv[cb, rows, :] for cb in range(4)]
        mean = jnp.sum(blocks[0] + blocks[1] + blocks[2] + blocks[3], axis=-1, keepdims=True) * (1.0 / 512)
        dev_sq = sum((b - mean) * (b - mean) for b in blocks)
        m2 = jnp.sum(dev_sq, axis=-1, keepdims=True)
        stat_own[rows, :] = jnp.where(low_lane[:64], mean, m2)
        return 0

    lax.fori_loop(0, 8, stats, 0)
    send(stat_own, stat_peer, stat_send.at[0], stat_recv.at[0], peer)

    all_colors(finish, 1, 2)

    def query_part(i, _):
        xi, s = i // 2, lax.rem(i, 2)
        full = project(s, xi, Q)
        for pair in (0, 1):
            v = full[:, pair * 128 : pair * 128 + 128]
            sq = v * v
            even = jnp.sum(jnp.where(low_lane, sq, 0.0), axis=-1, keepdims=True)
            odd = jnp.sum(jnp.where(low_lane, 0.0, sq), axis=-1, keepdims=True)
            scale = lax.rsqrt(jnp.where(low_lane, even, odd) * (1.0 / 64) + EPSILON)
            rounded = (v * scale * query_row).astype(BF).astype(F32) * 0.125
            qn[xi * 2 + pair, pl.ds(pl.multiple_of(s * 256, 256), 256), :] = rounded.astype(BF)
        return 0

    lax.fori_loop(0, 4, query_part, 0)
    all_colors(turn, 2, 2)

    row_i = lax.rem(lax.broadcasted_iota(jnp.int32, (256, 384), 0), 128)
    col_i = lax.broadcasted_iota(jnp.int32, (256, 384), 1)
    lane384 = lax.broadcasted_iota(jnp.int32, (384, 128), 1) < 64

    def attention(i, _):
        xi, s, b = i // 4, lax.rem(i // 2, 2), lax.rem(i, 2)
        base = pl.multiple_of(s * 256 + b * 128, 128)
        kv = kve[s, xi, pl.ds(pl.multiple_of(b * 128, 128), 384), :].astype(F32)
        swapped = pltpu.roll(kv, 64, 1)
        first = jnp.where(jnp.logical_and(is_first, s == 0), 128, 0) - b * 128
        end = jnp.where(jnp.logical_and(is_last, s == 1), 384, 512) - b * 128
        reach = col_i - row_i
        allowed = (reach >= 0) & (reach <= 256) & (col_i >= first) & (col_i < end)
        q01 = qn[xi * 2, pl.ds(base, 128), :].astype(F32)
        q23 = qn[xi * 2 + 1, pl.ds(base, 128), :].astype(F32)
        both = jnp.concatenate([q01, q23], axis=0)
        even = jnp.where(low_lane, both, 0.0).astype(BF)
        odd = jnp.where(low_lane, 0.0, both).astype(BF)
        nt = (((1,), (1,)), ((), ()))

        def mix(heads, keys, values):
            scores = lax.dot_general(heads, keys.astype(BF), nt, preferred_element_type=F32)
            weights = jnp.where(allowed, jnp.exp(scores), 0.0).astype(BF)
            return jnp.dot(weights, values.astype(BF), preferred_element_type=F32)

        o_even = mix(even, kv, jnp.where(lane384, swapped, 1.0))
        o_odd = mix(odd, swapped, jnp.where(lane384, 1.0, kv))
        number = jnp.where(low_lane, o_even, o_odd)
        weight = pltpu.roll(jnp.where(low_lane, o_odd, o_even), 64, 1)
        sink = jnp.exp(small[xi, 32:33, :])
        feats[xi, pl.ds(base, 128), 0:128] = (number[:128] / (weight[:128] + sink[:, :128])).astype(BF)
        feats[xi, pl.ds(base, 128), 128:256] = (number[128:] / (weight[128:] + sink[:, 128:])).astype(BF)
        return 0

    lax.fori_loop(0, 8, attention, 0)

    recv(stat_peer, stat_send.at[0], stat_recv.at[0])

    def feature(i, _):
        rows = pl.ds(pl.multiple_of(i * 64, 64), 64)
        a, b = stat_own[rows, :], stat_peer[rows, :]
        mean = 0.5 * (a[:, 0:1] + b[:, 0:1])
        gap = a[:, 0:1] - b[:, 0:1]
        spread = (a[:, 64:65] + b[:, 64:65] + gap * gap * 256.0) * (1.0 / 1024)
        scale = lax.rsqrt(spread + EPSILON)
        for cb in range(4):
            xi, half = cb // 2, cb % 2
            gain = small[xi, 31:32, half * 128 : half * 128 + 128]
            v = (conv[cb, rows, :] - mean) * scale * gain
            feats[xi, rows, 256 + half * 128 : 384 + half * 128] = (v * jax.nn.sigmoid(v)).astype(BF)
        return 0

    lax.fori_loop(0, 8, feature, 0)
    all_colors(finish, 2, 2)

    mine_rows = pl.ds(pl.multiple_of(k * 256, 256), 256)
    other_rows = pl.ds(pl.multiple_of((1 - k) * 256, 256), 256)
    for nb in range(8):
        zz, y0 = nb // 2, (nb % 2) * 2
        rhs = [jnp.concatenate([p[xi, zz, y0], p[xi, zz, y0 + 1]], axis=1) for xi in (0, 1)]
        part_send[nb] = sum(
            jnp.dot(feats[xi, other_rows, :], rhs[xi], preferred_element_type=F32) for xi in (0, 1)
        ).astype(BF)
        send(part_send.at[nb], part_recv.at[nb], out_send.at[nb], out_recv.at[nb], peer)
        part_own[nb] = sum(
            jnp.dot(feats[xi, mine_rows, :], rhs[xi], preferred_element_type=F32) for xi in (0, 1)
        )
    for nb in range(8):
        recv(part_recv.at[nb], out_send.at[nb], out_recv.at[nb])
        out[:, nb * 256 : nb * 256 + 256] = (part_own[nb] + part_recv[nb].astype(F32)).astype(BF)

    for src, dst, ssem, rsem, device, cond in sends:
        def done(src=src, dst=dst, ssem=ssem, rsem=rsem, device=device):
            copy(src, dst, ssem, rsem, device).wait_send()

        if cond is None:
            done()
        else:
            pl.when(cond)(done)


def on_device(tokens, mix_gain, wq, wk, wv, wcv, wcg, query_gain, key_gain, sinks, taps, conv_gain, attn_proj, conv_proj):
    vmem = pl.BlockSpec(memory_space=pltpu.VMEM)
    dma = pltpu.SemaphoreType.DMA
    return pl.pallas_call(
        kernel,
        out_shape=jax.ShapeDtypeStruct((256, 2048), BF),
        in_specs=[pl.BlockSpec(memory_space=pl.ANY)] + [vmem] * 13,
        out_specs=vmem,
        scratch_shapes=[
            pltpu.VMEM((2, 4, 4, 128, 896), BF),
            pltpu.VMEM((2, 4, 4, 512, 128), BF),
            pltpu.VMEM((64, 896), BF),
            pltpu.VMEM((256, 128), BF),
            pltpu.VMEM((256, 128), BF),
            pltpu.VMEM((2, 40, 256), F32),
            pltpu.VMEM((2, 4, 256, 512), BF),
            pltpu.VMEM((512, 2048), BF),
            pltpu.VMEM((4, 512, 128), BF),
            pltpu.VMEM((2, 2, 512, 128), BF),
            pltpu.VMEM((2, 4, 288, 128), F32),
            pltpu.VMEM((4, 512, 128), F32),
            pltpu.VMEM((512, 128), F32),
            pltpu.VMEM((512, 128), F32),
            pltpu.VMEM((2, 512, 512), BF),
            pltpu.VMEM((8, 256, 256), F32),
            pltpu.VMEM((8, 256, 256), BF),
            pltpu.VMEM((8, 256, 256), BF),
            dma((108,)), dma((108,)), dma((2,)), dma((2,)), dma((4,)), dma((4,)), dma((4,)), dma((4,)), dma(()),
            dma((4,)), dma((2,)), dma((8,)), dma((8,)), dma((1,)), dma((1,)), dma((8,)), dma((8,)),
        ],
        compiler_params=pltpu.CompilerParams(
            collective_id=0, has_side_effects=True, vmem_limit_bytes=60 * 1024 * 1024
        ),
        name="layer",
    )(
        tokens, mix_gain.reshape(1, -1), wq, wk, wv, wcv, wcg, query_gain.reshape(1, -1), key_gain.reshape(1, -1),
        jnp.repeat(sinks, 64).reshape(1, -1), taps, conv_gain.reshape(1, -1), attn_proj, conv_proj,
    )


def solution(mesh):
    placed = (
        P("sp", "tp"), P(), P("sp", "tp"), P("sp", "tp"), P("sp", "tp"), P("sp", "tp"), P("sp", "tp"),
        P(), P(), P("tp"), P(None, "tp"), P("tp"), P("tp", "sp"), P("tp", "sp"),
    )
    return jax.shard_map(
        on_device, mesh=mesh, in_specs=placed, out_specs=P(("sp", "tp"), None), check_vma=False
    )
```

time: 179 us -> 102 us (0.57)
  Pallas kernels: 0 us -> 96.1 us
  waiting for transfers between devices: 64.3 us -> 0 us
  blocking collectives: 29.6 us -> 0 us
  other arithmetic: 22.6 us -> 0 us
  matrix products: 18.8 us -> 0 us
  starting transfers between devices: 17.3 us -> 0 us
  between operations: 14.3 us -> 0.01 us
  local copies, waits for them, and re-layouts: 11.1 us -> 5.92 us
    pallas_call x0 -> x1, Pallas kernels: none -> 96.1 us  [on_device(): pl.pallas_call(kernel, out_shape=jax.ShapeDtypeStruct((256, 2048), BF), i...]
    all_gather x2 -> x0, waiting for transfers between devices: 60 us -> none  [the longest x1 40.3 us: on_device(): lax.all_gather(jnp.concatenate([wq, wk, wv, wcv, wcg], axis=1), ('tp', 's...]
    dot_general x4 -> x0, matrix products: 18.8 us -> none  [the longest x1 7.26 us: on_device(): jnp.einsum('tk,pkc->tpc', normed, w_in, preferred_element_type=jnp.float32)]
    all_gather x2 -> x0, blocking collectives: 16.9 us -> none  [the longest x1 9.43 us: on_device(): lax.all_gather(taps, 'tp')]
    reduce_sum x5 -> x0, other arithmetic: 15.3 us -> none  [the longest x1 14.5 us: on_device(): center = jnp.mean(convolved, axis=1, keepdims=True)]
    unnamed x1 -> x0, blocking collectives: 12.7 us -> none
    ppermute x4 -> x0, starting transfers between devices: 12.4 us -> none  [the longest x2 7.19 us: halo(): after = lax.ppermute(value[:width], BOTH, down)]
    all_to_all x1 -> x0, starting transfers between devices: 4.84 us -> none  [on_device(): lax.all_to_all(tokens.reshape(tps, count, -1), 'tp', 0, 0, tiled=True)]
  transfers between devices with their start and end apart: 7 -> 0, of which waited for: 3 -> 0; matrix products, arithmetic and copies ran while one was open for 24% -> 0% of each run, Pallas kernels for 0% -> 0%
where the time goes in v2:
time: 102 us
  Pallas kernels  96.1 us (94%)
  local copies, waits for them, and re-layouts  5.92 us (6%)
    pallas_call x1, Pallas kernels, on_device(): pl.pallas_call(kernel, out_shape=jax.ShapeDtypeStruct((256, 2048), BF), i...  96.1 us
    unnamed x7, local copies, waits for them, and re-layouts  5.19 us

profile of v2, /device:TPU:1, one launch (start us, length us, event | category | flops | bytes accessed | tf_op | source)
XLA Modules:
  0.0 102.1 jit_solution(15712595299918114133)
XLA Ops:
  0.0 0.0 copy-start.1
  0.0 0.7 copy-done.1
  0.7 0.1 broadcast_in_dim.3
  0.7 0.7 reshape_reshape.3.sink_row
  1.4 0.0 copy-start
  1.4 1.5 %copy.15.attn_proj = bf16[256,64]{1,0:T(8,128)(2,1)} copy(bf16[256,64]{0,1:T(8,128)(2,1)} %param.26) | data formatting | bytes 65536 | tf_op args[12]
  2.9 0.0 copy-done
  2.9 0.7 copy.16.conv_proj
  3.6 96.1 %layer.1 = bf16[256,2048]{1,0:T(8,128)(2,1)} custom-call(bf16[1024,512]{1,0:T(8,128)(2,1)} %tokens.1, f32[1,2048]{1,0:T(1,128)} %bitcast.4, bf16[64,256]{1,0:T(8,128)(2,1)} %wq.1, bf16[64,64]{1,0:T(8,128)(2,1)} %wk.1, bf16[64,64]{1,0:T(8,128)(2,1)} %wv.1, bf16[64,256]{1,0:T(8,128)(2,1)} %wcv.1, bf16[64,256]{1,0:T(8,128)(2,1)} %wcg.1, f32[1,64]{1,0:T(1,128)} %bitcast.6, ...), custom_call_target="tpu_custom_call" | custom-call | tf_op jit(solution)/shard_map/layer/pallas_call | solution.py:459
  99.8 2.3 %copy.18 = bf16[256,2048]{1,0:T(8,128)(2,1)} copy(bf16[256,2048]{1,0:T(8,128)(2,1)} %layer.1) | data formatting | bytes 2097152
Async XLA Ops:
  0.0 0.7 copy-start.1
  1.4 1.5 %copy-start = (bf16[256,64]{0,1:T(8,128)(2,1)S(1)}, bf16[256,64]{0,1:T(8,128)(2,1)}, u32[]{:S(2)}) copy-start(bf16[256,64]{0,1:T(8,128)(2,1)} %param.27) | copy-start | bytes 98308

commit v3 on v2

--- a/solution.py
+++ b/solution.py
@@ -10,23 +10,29 @@
 BF = jnp.bfloat16
 F32 = jnp.float32
 
-CV, CG, KV, Q = (0, 256), (256, 512), (512, 640), (640, 896)
+CV, CG, Q, KV = (0, 256), (256, 512), (512, 768), (768, 896)
 STAGES = (
-    ("w", 0, 640, ((0, 48, 32), (48, 32, 16), (80, 48, 32))),
-    ("w", 640, 256, ((0, 32, 16), (32, 48, 32), (80, 48, 32))),
-    ("p", 0, 128, ((0, 176, 96), (176, 160, 80), (336, 176, 96))),
+    ("w", 0, 512, ((0, 48, 32), (48, 32, 16), (80, 48, 32))),
+    ("w", 512, 384, ((0, 48, 32), (48, 32, 16), (80, 48, 32))),
+    ("p", 0, 128, ((0, 144, 80), (144, 176, 96), (320, 192, 96))),
 )
-ORDERS = ("xyz", "yzx", "zxy")
+ORDERS = ("xyz", "yzx", "xzy")
 
 
 def kernel(
-    tokens, mix_gain, wq, wk, wv, wcv, wcg, query_gain, key_gain, sink_row, taps, conv_gain, attn_proj, conv_proj,
-    out,
-    w, p, mine_w, mine_p, peer_p, small, x_buf, normed, qn, kve, ge, conv, stat_own, stat_peer, feats,
-    part_own, part_send, part_recv,
-    ag_send, ag_recv, d2d_send, d2d_recv, tok_send, tok_recv, fwd_send, fwd_recv, loc_sem, sm_send, sm_recv,
-    halo_send, halo_recv, stat_send, stat_recv, out_send, out_recv,
+    tokens, *rest,
 ):
+    given, (out, *held), rest = rest[:13], rest[13:27], rest[27:]
+    mix_gain, wq, wk, wv, wcv, wcg, query_gain, key_gain, sinks, taps, conv_gain, attn_proj, conv_proj = held
+    (
+        w, p, mine_w, mine_p, peer_p, small, hop, edge_send, edge_recv, x_buf, normed, qn, kve, ge, conv, stat_own,
+        stat_peer, feats, part_own, part_send, part_recv,
+        load_sem, ag_send, ag_recv, d2d_send, d2d_recv, tok_send, tok_recv, hop_send, hop_recv, fwd_send, fwd_recv,
+        loc_sem, sm_send, sm_recv, halo_send, halo_recv, stat_send, stat_recv, out_send, out_recv,
+    ) = rest
+    loads = [pltpu.make_async_copy(a, b, load_sem.at[i]) for i, (a, b) in enumerate(zip(given, held))]
+    for load in loads:
+        load.start()
     sp, x = lax.axis_index("sp"), lax.axis_index("tp")
     k = lax.rem(sp, 2)
     q = sp // 2
@@ -93,8 +99,8 @@
             if axis == "z":
                 return buf.at[xi0, where, two[half], rr, cols]
             return buf.at[where, two[half], :, rr, cols]
-        if axis == "x":
-            return buf.at[where, two[half], y, rr, cols]
+        if axis == "z":
+            return buf.at[one[half], where, y, rr, cols]
         return buf.at[one[half], :, where, rr, cols]
 
     def context(stage, color, phase):
@@ -156,8 +162,33 @@
         for color in range(3):
             step(stage, color, phase)
 
+    def flush(count=None):
+        for _ in range(len(sends) if count is None else count):
+            src, dst, ssem, rsem, device, cond = sends.pop(0)
+
+            def done():
+                copy(src, dst, ssem, rsem, device).wait_send()
+
+            if cond is None:
+                done()
+            else:
+                pl.when(cond)(done)
+
     own_rows = pl.ds(pl.multiple_of(k * 64, 64), 64)
-    shard = jnp.concatenate([wcv[...], wcg[...], wk[...], wv[...], wq[...]], axis=1)
+    barrier = pltpu.get_barrier_semaphore()
+    y_up, z_up = up(y), up(z)
+    partners = [
+        peer, dev(up(x), y, z, k), dev(up(x, 3), y, z, k),
+        dev(x, y_up, z, k), dev(x, up(y, 3), z, k), dev(x, y, z_up, k), dev(x, y, up(z, 3), k),
+    ]
+    for partner in partners:
+        pl.semaphore_signal(barrier, inc=1, device_id=partner, device_id_type=MESH)
+    own = pl.multiple_of(x * 256, 256)
+    local = pltpu.make_async_copy(tokens.at[pl.ds(own, 256), :], x_buf.at[k, x], loc_sem)
+    local.start()
+    for load in loads:
+        load.wait()
+    shard = jnp.concatenate([wcv[...], wcg[...], wq[...], wk[...], wv[...]], axis=1)
 
     @pl.when(is_source)
     def _():
@@ -167,21 +198,13 @@
     def _():
         mine_w[...] = shard
 
-    mine_p[...] = jnp.concatenate([attn_proj[...], conv_proj[...]], axis=1)
+    mine_p[...] = jnp.concatenate([attn_proj[...], conv_proj[...]], axis=0)
     small[xi0, 0:31, :] = taps[...]
     small[xi0, 31:32, :] = conv_gain[...]
-    small[xi0, 32:33, :] = sink_row[...]
-
-    barrier = pltpu.get_barrier_semaphore()
-    y_up, z_up = up(y), up(z)
-    q_next, q_last = lax.rem(q + 1, 16), lax.rem(q + 15, 16)
-    partners = [
-        peer, dev(up(x), y, z, k), dev(up(x, 2), y, z, k), dev(up(x, 3), y, z, k),
-        dev(x, y_up, z, k), dev(x, up(y, 3), z, k), dev(x, y, z_up, k), dev(x, y, up(z, 3), k),
-        (q_next * 2 + k, up(x)), (q_last * 2 + k, up(x, 3)),
-    ]
-    for partner in partners:
-        pl.semaphore_signal(barrier, inc=1, device_id=partner, device_id_type=MESH)
+    small[xi0, 32:33, :] = jnp.concatenate(
+        [jnp.broadcast_to(sinks[:, h : h + 1], (1, 64)) for h in range(4)], axis=1
+    )
+
     pl.semaphore_wait(barrier, len(partners))
 
     not_source = jnp.logical_not(is_source)
@@ -191,23 +214,34 @@
     peer_rows = pl.ds(pl.multiple_of((1 - k) * 64, 64), 64)
     recv(w.at[xi0, z, y, peer_rows, :], d2d_send.at[0], d2d_recv.at[0], is_source)
     all_colors(start1, 0, 0)
-
-    for d in (1, 3, 2):
-        to = up(x, d)
-        rows = pl.ds(pl.multiple_of(to * 256, 256), 256)
-        send(tokens.at[rows, :], x_buf.at[k, x], tok_send.at[d], tok_recv.at[d], dev(to, y, z, k))
-    rows = pl.ds(pl.multiple_of(x * 256, 256), 256)
-    local = pltpu.make_async_copy(tokens.at[rows, :], x_buf.at[k, x], loc_sem)
-    local.start()
-    send(tokens.at[rows, :], x_buf.at[k, x], fwd_send.at[0], fwd_recv.at[0], peer)
-    mine_small = small.at[xi0]
-    for d in (1, 2, 3):
-        send(mine_small, mine_small, sm_send.at[d], sm_recv.at[xi0], dev(up(x, d), y, z, k), is_source)
-
-    all_colors(turn, 0, 0)
     all_colors(start1, 1, 0)
-    all_colors(finish, 0, 0)
-    all_colors(start1, 0, 1)
+
+    right, left, across = dev(up(x), y, z, k), dev(up(x, 3), y, z, k), up(x, 2)
+
+    def token_sends():
+        for to, device, i in ((up(x), right, 0), (up(x, 3), left, 1)):
+            far = tokens.at[pl.ds(pl.multiple_of(across * 256 + i * 128, 128), 128), :]
+            send(far, hop.at[i], hop_send.at[i], hop_recv.at[i], device)
+            near = tokens.at[pl.ds(pl.multiple_of(to * 256, 256), 256), :]
+            send(near, x_buf.at[k, x], tok_send.at[i], tok_recv.at[i], device)
+
+    def token_hops():
+        for origin, device, i in ((up(x, 3), right, 0), (up(x), left, 1)):
+            recv(hop.at[i], hop_send.at[i], hop_recv.at[i])
+            send(hop.at[i], x_buf.at[k, origin, pl.ds(i * 128, 128), :], tok_send.at[2 + i], tok_recv.at[2 + i], device)
+
+    def tokens_on():
+        for i, origin in ((0, up(x, 3)), (1, up(x))):
+            recv(x_buf.at[k, origin], tok_send.at[i], tok_recv.at[i])
+            send(x_buf.at[k, origin], x_buf.at[k, origin], fwd_send.at[1 + i], fwd_recv.at[1 + i], peer)
+        for i in (0, 1):
+            recv(x_buf.at[k, across, pl.ds(i * 128, 128), :], tok_send.at[2 + i], tok_recv.at[2 + i])
+        send(x_buf.at[k, across], x_buf.at[k, across], fwd_send.at[3], fwd_recv.at[3], peer)
+
+    def small_on():
+        recv(small.at[1 - xi0], sm_send.at[0], sm_recv.at[1 - xi0])
+        beyond = dev(jnp.where(jnp.logical_or(pos == 0, pos == 3), up(x, 3), up(x)), y, z, k)
+        send(small.at[1 - xi0], small.at[1 - xi0], sm_send.at[2], sm_recv.at[1 - xi0], beyond, is_source)
 
     recv(peer_p, d2d_send.at[1], d2d_recv.at[1])
 
@@ -216,31 +250,37 @@
         a, b = mine_p[...], peer_p[...]
         low = jnp.where(k == 0, a, b)
         high = jnp.where(k == 0, b, a)
-        p[xi0, z, y, 0:256, :] = jnp.concatenate([low[:, :64], high[:, :64]], axis=1)
-        p[xi0, z, y, 256:512, :] = jnp.concatenate([low[:, 64:], high[:, 64:]], axis=1)
-
+        p[xi0, z, y, 0:256, :] = jnp.concatenate([low[:64], high[:64]], axis=0).T
+        p[xi0, z, y, 256:512, :] = jnp.concatenate([low[64:], high[64:]], axis=0).T
+
+    all_colors(turn, 0, 0)
     all_colors(turn, 1, 0)
+    all_colors(start1, 2, 0)
+    token_sends()
+    send(tokens.at[pl.ds(own, 256), :], x_buf.at[k, x], fwd_send.at[0], fwd_recv.at[0], peer)
+    mine_small = small.at[xi0]
+    for i, device in enumerate((right, left)):
+        send(mine_small, mine_small, sm_send.at[i], sm_recv.at[xi0], device, is_source)
+    all_colors(finish, 0, 0)
+    all_colors(start1, 0, 1)
+    all_colors(finish, 1, 0)
+    all_colors(start1, 1, 1)
+    all_colors(turn, 2, 0)
     all_colors(turn, 0, 1)
-    all_colors(finish, 1, 0)
-    all_colors(finish, 0, 1)
-    all_colors(start1, 0, 2)
-    all_colors(start1, 1, 1)
-    all_colors(start1, 2, 0)
-
-    for d in (1, 3, 2):
-        origin = up(x, 4 - d)
-        recv(x_buf.at[k, origin], tok_send.at[d], tok_recv.at[d])
-        send(x_buf.at[k, origin], x_buf.at[k, origin], fwd_send.at[d], fwd_recv.at[d], peer)
-
-    all_colors(turn, 2, 0)
     all_colors(turn, 1, 1)
     all_colors(finish, 2, 0)
+    all_colors(start1, 2, 1)
+    token_hops()
+    all_colors(finish, 0, 1)
+    early = len(sends)
+    all_colors(start1, 0, 2)
+    small_on()
     all_colors(finish, 1, 1)
-
+    tokens_on()
     local.wait()
     recv(x_buf.at[1 - k, x], fwd_send.at[0], fwd_recv.at[0])
-    for d in (1, 3, 2):
-        recv(x_buf.at[1 - k, up(x, 4 - d)], fwd_send.at[d], fwd_recv.at[d])
+    for i, origin in ((1, up(x, 3)), (2, up(x)), (3, across)):
+        recv(x_buf.at[1 - k, origin], fwd_send.at[i], fwd_recv.at[i])
 
     def norm_rows(i, _):
         s, r = i // 8, lax.rem(i, 8)
@@ -257,8 +297,9 @@
     lax.fori_loop(0, 16, norm_rows, 0)
 
     all_colors(turn, 0, 2)
+    all_colors(turn, 2, 1)
     all_colors(start1, 1, 2)
-    all_colors(start1, 2, 1)
+    flush(early)
     all_colors(finish, 0, 2)
 
     lane = lax.broadcasted_iota(jnp.int32, (256, 128), 1)
@@ -271,52 +312,40 @@
         rhs = w[xi, :, :, :, cols[0] : cols[1]].reshape(2048, cols[1] - cols[0])
         return jnp.dot(lhs, rhs, preferred_element_type=F32)
 
-    def first_part(i, _):
+    def gated_part(i, _):
         xi, s = i // 2, lax.rem(i, 2)
-        kv = project(s, xi, KV)
-        square = jnp.sum(jnp.where(low_lane, kv * kv, 0.0), axis=-1, keepdims=True)
-        keyed = kv * lax.rsqrt(square * (1.0 / 64) + EPSILON) * key_row
-        kve[s, xi, 128:384, :] = jnp.where(low_lane, keyed, kv).astype(BF)
         value, gate = project(s, xi, CV), project(s, xi, CG)
-        gated = (value * jax.nn.sigmoid(gate)).astype(BF).astype(F32)
-        ge[s, xi * 2, 16:272, :] = gated[:, :128]
-        ge[s, xi * 2 + 1, 16:272, :] = gated[:, 128:]
-        return 0
-
-    lax.fori_loop(0, 4, first_part, 0)
-
-    for s in (0, 1):
-        for side in (0, 1):
-            if side == 0:
-                wraps = x == 3
-                step = jnp.where(jnp.logical_and(wraps, s == 1), 1, 0)
-                to = (lax.rem(q + step, 16) * 2 + k, up(x))
-                src_kv, dst_kv, src_ge, dst_ge = (256, 0, 256, 0)
-            else:
-                wraps = x == 0
-                step = jnp.where(jnp.logical_and(wraps, s == 0), 15, 0)
-                to = (lax.rem(q + step, 16) * 2 + k, up(x, 3))
-                src_kv, dst_kv, src_ge, dst_ge = (128, 384, 16, 272)
-            seg = jnp.where(wraps, 1 - s, s)
-            i = s * 4 + side * 2
-            j = seg * 4 + side * 2
-            send(kve.at[s, :, pl.ds(src_kv, 128), :], kve.at[seg, :, pl.ds(dst_kv, 128), :],
-                 halo_send.at[i], halo_recv.at[j], to)
-            send(ge.at[s, :, pl.ds(src_ge, 16), :], ge.at[seg, :, pl.ds(dst_ge, 16), :],
-                 halo_send.at[i + 1], halo_recv.at[j + 1], to)
-
-    all_colors(turn, 2, 1)
-    all_colors(turn, 1, 2)
-    all_colors(finish, 2, 1)
-    all_colors(start1, 2, 2)
-
-    for s in (0, 1):
-        for side in (0, 1):
-            i = s * 4 + side * 2
-            recv(kve.at[s, :, pl.ds(0 if side == 0 else 384, 128), :], halo_send.at[i], halo_recv.at[i])
-            recv(ge.at[s, :, pl.ds(0 if side == 0 else 272, 16), :], halo_send.at[i + 1], halo_recv.at[i + 1])
+        rounded = (value * jax.nn.sigmoid(gate)).astype(BF)
+        gated = rounded.astype(F32)
+        for half in (0, 1):
+            lanes = slice(half * 128, half * 128 + 128)
+            ge[s, xi * 2 + half, 16:272, :] = gated[:, lanes]
+            edge_send[s, 0, xi * 2 + half] = rounded[240:, lanes]
+            edge_send[s, 1, xi * 2 + half] = rounded[:16, lanes]
+        return 0
+
+    lax.fori_loop(0, 4, gated_part, 0)
+
+    def neighbour(s, side):
+        wraps, over = (x == 3, 1) if side == 0 else (x == 0, 15)
+        step = jnp.where(jnp.logical_and(wraps, s == 1 - side), over, 0)
+        return (lax.rem(q + step, 16) * 2 + k, up(x, 1 if side == 0 else 3)), jnp.where(wraps, 1 - s, s)
+
+    SIDES = ((0, 0), (0, 1), (1, 0), (1, 1))
     is_first = jnp.logical_and(q == 0, x == 0)
     is_last = jnp.logical_and(q == 15, x == 3)
+
+    for s, side in SIDES:
+        to, seg = neighbour(s, side)
+        send(edge_send.at[s, side], edge_recv.at[seg, side], halo_send.at[4 + s * 2 + side],
+             halo_recv.at[4 + seg * 2 + side], to)
+    all_colors(finish, 2, 1)
+    all_colors(turn, 1, 2)
+    all_colors(start1, 2, 2)
+    recv(small.at[xi0], sm_send.at[0], sm_recv.at[xi0], not_source)
+    for s, side in SIDES:
+        recv(edge_recv.at[s, side], halo_send.at[4], halo_recv.at[4 + s * 2 + side])
+        ge[s, :, side * 272 : side * 272 + 16, :] = edge_recv[s, side].astype(F32)
 
     @pl.when(is_first)
     def _():
@@ -325,9 +354,6 @@
     @pl.when(is_last)
     def _():
         ge[1, :, 272:288, :] = jnp.zeros((4, 16, 128), F32)
-
-    recv(small.at[1 - xi0], sm_send.at[1], sm_recv.at[1 - xi0])
-    recv(small.at[xi0], sm_send.at[1], sm_recv.at[xi0], not_source)
 
     def conv_block(i, _):
         s, cb = i // 4, lax.rem(i, 4)
@@ -356,6 +382,20 @@
 
     all_colors(finish, 1, 2)
 
+    def first_part(i, _):
+        xi, s = i // 2, lax.rem(i, 2)
+        kv = project(s, xi, KV)
+        square = jnp.sum(jnp.where(low_lane, kv * kv, 0.0), axis=-1, keepdims=True)
+        keyed = kv * lax.rsqrt(square * (1.0 / 64) + EPSILON) * key_row
+        kve[s, xi, 128:384, :] = jnp.where(low_lane, keyed, kv).astype(BF)
+        return 0
+
+    lax.fori_loop(0, 4, first_part, 0)
+    for s, side in SIDES:
+        to, seg = neighbour(s, side)
+        src, dst = (256, 0) if side == 0 else (128, 384)
+        send(kve.at[s, :, pl.ds(src, 128), :], kve.at[seg, :, pl.ds(dst, 128), :],
+             halo_send.at[s * 2 + side], halo_recv.at[seg * 2 + side], to)
     def query_part(i, _):
         xi, s = i // 2, lax.rem(i, 2)
         full = project(s, xi, Q)
@@ -370,7 +410,26 @@
         return 0
 
     lax.fori_loop(0, 4, query_part, 0)
+    recv(stat_peer, stat_send.at[0], stat_recv.at[0])
+
+    def feature(i, _):
+        rows = pl.ds(pl.multiple_of(i * 64, 64), 64)
+        a, b = stat_own[rows, :], stat_peer[rows, :]
+        mean = 0.5 * (a[:, 0:1] + b[:, 0:1])
+        gap = a[:, 0:1] - b[:, 0:1]
+        spread = (a[:, 64:65] + b[:, 64:65] + gap * gap * 256.0) * (1.0 / 1024)
+        scale = lax.rsqrt(spread + EPSILON)
+        for cb in range(4):
+            xi, half = cb // 2, cb % 2
+            gain = small[xi, 31:32, half * 128 : half * 128 + 128]
+            v = (conv[cb, rows, :] - mean) * scale * gain
+            feats[rows, xi * 512 + 256 + half * 128 : xi * 512 + 384 + half * 128] = (v * jax.nn.sigmoid(v)).astype(BF)
+        return 0
+
+    lax.fori_loop(0, 8, feature, 0)
     all_colors(turn, 2, 2)
+    for s, side in SIDES:
+        recv(kve.at[s, :, pl.ds(0 if side == 0 else 384, 128), :], halo_send.at[0], halo_recv.at[s * 2 + side])
 
     row_i = lax.rem(lax.broadcasted_iota(jnp.int32, (256, 384), 0), 128)
     col_i = lax.broadcasted_iota(jnp.int32, (256, 384), 1)
@@ -402,72 +461,53 @@
         number = jnp.where(low_lane, o_even, o_odd)
         weight = pltpu.roll(jnp.where(low_lane, o_odd, o_even), 64, 1)
         sink = jnp.exp(small[xi, 32:33, :])
-        feats[xi, pl.ds(base, 128), 0:128] = (number[:128] / (weight[:128] + sink[:, :128])).astype(BF)
-        feats[xi, pl.ds(base, 128), 128:256] = (number[128:] / (weight[128:] + sink[:, 128:])).astype(BF)
+        col = pl.multiple_of(xi * 512, 512)
+        feats[pl.ds(base, 128), pl.ds(col, 128)] = (number[:128] / (weight[:128] + sink[:, :128])).astype(BF)
+        feats[pl.ds(base, 128), pl.ds(col + 128, 128)] = (number[128:] / (weight[128:] + sink[:, 128:])).astype(BF)
         return 0
 
     lax.fori_loop(0, 8, attention, 0)
 
-    recv(stat_peer, stat_send.at[0], stat_recv.at[0])
-
-    def feature(i, _):
-        rows = pl.ds(pl.multiple_of(i * 64, 64), 64)
-        a, b = stat_own[rows, :], stat_peer[rows, :]
-        mean = 0.5 * (a[:, 0:1] + b[:, 0:1])
-        gap = a[:, 0:1] - b[:, 0:1]
-        spread = (a[:, 64:65] + b[:, 64:65] + gap * gap * 256.0) * (1.0 / 1024)
-        scale = lax.rsqrt(spread + EPSILON)
-        for cb in range(4):
-            xi, half = cb // 2, cb % 2
-            gain = small[xi, 31:32, half * 128 : half * 128 + 128]
-            v = (conv[cb, rows, :] - mean) * scale * gain
-            feats[xi, rows, 256 + half * 128 : 384 + half * 128] = (v * jax.nn.sigmoid(v)).astype(BF)
-        return 0
-
-    lax.fori_loop(0, 8, feature, 0)
     all_colors(finish, 2, 2)
 
-    mine_rows = pl.ds(pl.multiple_of(k * 256, 256), 256)
-    other_rows = pl.ds(pl.multiple_of((1 - k) * 256, 256), 256)
     for nb in range(8):
         zz, y0 = nb // 2, (nb % 2) * 2
-        rhs = [jnp.concatenate([p[xi, zz, y0], p[xi, zz, y0 + 1]], axis=1) for xi in (0, 1)]
-        part_send[nb] = sum(
-            jnp.dot(feats[xi, other_rows, :], rhs[xi], preferred_element_type=F32) for xi in (0, 1)
-        ).astype(BF)
-        send(part_send.at[nb], part_recv.at[nb], out_send.at[nb], out_recv.at[nb], peer)
-        part_own[nb] = sum(
-            jnp.dot(feats[xi, mine_rows, :], rhs[xi], preferred_element_type=F32) for xi in (0, 1)
+        rhs = jnp.concatenate(
+            [jnp.concatenate([p[xi, zz, y0], p[xi, zz, y0 + 1]], axis=1) for xi in (0, 1)], axis=0
         )
+        part = jnp.dot(feats[...], rhs, preferred_element_type=F32).reshape(2, 256, 256)
+        part_send[nb] = part.astype(BF)
+        send(part_send.at[nb, 1 - k], part_recv.at[nb], out_send.at[nb], out_recv.at[nb], peer)
+        part_own[nb] = part
     for nb in range(8):
         recv(part_recv.at[nb], out_send.at[nb], out_recv.at[nb])
-        out[:, nb * 256 : nb * 256 + 256] = (part_own[nb] + part_recv[nb].astype(F32)).astype(BF)
-
-    for src, dst, ssem, rsem, device, cond in sends:
-        def done(src=src, dst=dst, ssem=ssem, rsem=rsem, device=device):
-            copy(src, dst, ssem, rsem, device).wait_send()
-
-        if cond is None:
-            done()
-        else:
-            pl.when(cond)(done)
+        out[:, nb * 256 : nb * 256 + 256] = (part_own[nb, k] + part_recv[nb].astype(F32)).astype(BF)
+    flush()
 
 
 def on_device(tokens, mix_gain, wq, wk, wv, wcv, wcg, query_gain, key_gain, sinks, taps, conv_gain, attn_proj, conv_proj):
     vmem = pl.BlockSpec(memory_space=pltpu.VMEM)
     dma = pltpu.SemaphoreType.DMA
+    arrays = (
+        tokens, mix_gain.reshape(1, -1), wq, wk, wv, wcv, wcg, query_gain.reshape(1, -1), key_gain.reshape(1, -1),
+        sinks.reshape(1, -1), taps, conv_gain.reshape(1, -1), attn_proj.T, conv_proj.T,
+    )
     return pl.pallas_call(
         kernel,
         out_shape=jax.ShapeDtypeStruct((256, 2048), BF),
-        in_specs=[pl.BlockSpec(memory_space=pl.ANY)] + [vmem] * 13,
+        in_specs=[pl.BlockSpec(memory_space=pltpu.HBM)] * 14,
         out_specs=vmem,
         scratch_shapes=[
+            *(pltpu.VMEM(a.shape, a.dtype) for a in arrays[1:]),
             pltpu.VMEM((2, 4, 4, 128, 896), BF),
             pltpu.VMEM((2, 4, 4, 512, 128), BF),
             pltpu.VMEM((64, 896), BF),
-            pltpu.VMEM((256, 128), BF),
-            pltpu.VMEM((256, 128), BF),
+            pltpu.VMEM((128, 256), BF),
+            pltpu.VMEM((128, 256), BF),
             pltpu.VMEM((2, 40, 256), F32),
+            pltpu.VMEM((2, 128, 512), BF),
+            pltpu.VMEM((2, 2, 4, 16, 128), BF),
+            pltpu.VMEM((2, 2, 4, 16, 128), BF),
             pltpu.VMEM((2, 4, 256, 512), BF),
             pltpu.VMEM((512, 2048), BF),
             pltpu.VMEM((4, 512, 128), BF),
@@ -476,21 +516,18 @@
             pltpu.VMEM((4, 512, 128), F32),
             pltpu.VMEM((512, 128), F32),
             pltpu.VMEM((512, 128), F32),
-            pltpu.VMEM((2, 512, 512), BF),
-            pltpu.VMEM((8, 256, 256), F32),
+            pltpu.VMEM((512, 1024), BF),
+            pltpu.VMEM((8, 2, 256, 256), F32),
+            pltpu.VMEM((8, 2, 256, 256), BF),
             pltpu.VMEM((8, 256, 256), BF),
-            pltpu.VMEM((8, 256, 256), BF),
-            dma((108,)), dma((108,)), dma((2,)), dma((2,)), dma((4,)), dma((4,)), dma((4,)), dma((4,)), dma(()),
+            dma((13,)), dma((108,)), dma((108,)), dma((2,)), dma((2,)), dma((4,)), dma((4,)), dma((2,)), dma((2,)), dma((4,)), dma((4,)), dma(()),
             dma((4,)), dma((2,)), dma((8,)), dma((8,)), dma((1,)), dma((1,)), dma((8,)), dma((8,)),
         ],
         compiler_params=pltpu.CompilerParams(
-            collective_id=0, has_side_effects=True, vmem_limit_bytes=60 * 1024 * 1024
+            collective_id=0, has_side_effects=True, vmem_limit_bytes=62 * 1024 * 1024
         ),
         name="layer",
-    )(
-        tokens, mix_gain.reshape(1, -1), wq, wk, wv, wcv, wcg, query_gain.reshape(1, -1), key_gain.reshape(1, -1),
-        jnp.repeat(sinks, 64).reshape(1, -1), taps, conv_gain.reshape(1, -1), attn_proj, conv_proj,
-    )
+    )(*arrays)
 
 
 def solution(mesh):

time: 102 us -> 88.7 us (0.87)
  Pallas kernels: 96.1 us -> 86.2 us
  local copies, waits for them, and re-layouts: 5.92 us -> 2.3 us
    pallas_call x1, Pallas kernels: 96.1 us -> 86.2 us  [on_device(): pl.pallas_call(kernel, out_shape=jax.ShapeDtypeStruct((256, 2048), BF), i...]
    unnamed x7 -> x1, local copies, waits for them, and re-layouts: 5.19 us -> 2.3 us
where the time goes in v3:
time: 88.7 us; the launch traced here: 88.5 us
  Pallas kernels  86.2 us (97%)
  local copies, waits for them, and re-layouts  2.3 us (3%)
    pallas_call x1, Pallas kernels, on_device(): pl.pallas_call(kernel, out_shape=jax.ShapeDtypeStruct((256, 2048), BF), i...  86.2 us
    unnamed x1, local copies, waits for them, and re-layouts  2.3 us

profile of v3, /device:TPU:1, one launch (start us, length us, event | category | flops | bytes accessed | tf_op | source)
XLA Modules:
  0.0 88.5 jit_solution(5492138411771800843)
XLA Ops:
  0.0 86.2 %layer.1 = bf16[256,2048]{1,0:T(8,128)(2,1)} custom-call(bf16[1024,512]{1,0:T(8,128)(2,1)} %tokens.1, f32[1,2048]{1,0:T(1,128)} %bitcast.9, bf16[64,256]{1,0:T(8,128)(2,1)} %rest_1_.1, bf16[64,64]{1,0:T(8,128)(2,1)} %rest_2_.1, bf16[64,64]{1,0:T(8,128)(2,1)} %rest_3_.1, bf16[64,256]{1,0:T(8,128)(2,1)} %rest_4_.1, bf16[64,256]{1,0:T(8,128)(2,1)} %rest_5_.1, ...), custom_call_target="tpu_custom_call" | custom-call | tf_op jit(solution)/shard_map/layer/pallas_call | solution.py:495
  86.2 2.3 %copy.16 = bf16[256,2048]{1,0:T(8,128)(2,1)} copy(bf16[256,2048]{1,0:T(8,128)(2,1)} %layer.1) | data formatting | bytes 2097152

commit v4 on v3

v4 whole, which is shorter than its diff:
```python
import jax
import jax.numpy as jnp
from jax import lax
from jax.experimental import pallas as pl
from jax.experimental.pallas import tpu as pltpu
from jax.sharding import PartitionSpec as P

MESH = pl.DeviceIdType.MESH
EPSILON = 0.1
BF = jnp.bfloat16
F32 = jnp.float32

CV, CG, Q, KV = (0, 256), (256, 512), (512, 768), (768, 896)
STAGES = (
    ("w", 0, 512, ((0, 48, 32), (48, 32, 16), (80, 48, 32))),
    ("w", 512, 384, ((0, 48, 32), (48, 32, 16), (80, 48, 32))),
    ("p", 0, 128, ((0, 176, 96), (176, 160, 80), (336, 176, 96))),
)
ORDERS = ("xyz", "yzx", "zxy")
SLOTS = {(False, True): range(2), (False, False): range(3), (True, True): range(4), (True, False): range(6)}
SLOT_COUNT = 3 * sum(
    len(SLOTS[phase > 0, axis == "x"]) for order in ORDERS for phase, axis in enumerate(order)
)
POOL = 112


def kernel(
    tokens, *rest,
):
    given, (out, *held), rest = rest[:13], rest[13:27], rest[27:]
    mix_gain, wq, wk, wv, wcv, wcg, query_gain, key_gain, sinks, taps, conv_gain, attn_proj, conv_proj = held
    (
        w, p, mine_w, mine_p, peer_p, small, hop, edge_send, edge_recv, x_buf, normed, qn, kve, ge, conv, stat_own,
        stat_peer, feats, part_own, part_send, part_recv,
        load_sem, pool, ag_recv, d2d_recv, tok_recv, hop_recv, fwd_recv, loc_sem, sm_recv, halo_recv, stat_recv,
        out_recv,
    ) = rest
    loads = [pltpu.make_async_copy(a, b, load_sem.at[i]) for i, (a, b) in enumerate(zip(given, held))]
    for load in loads:
        load.start()
    sp, x = lax.axis_index("sp"), lax.axis_index("tp")
    k = lax.rem(sp, 2)
    q = sp // 2
    y, z = lax.rem(q, 4), q // 4
    pos = lax.rem(x + 4 - 2 * k, 4)
    xi0 = lax.rem(x, 2)
    is_source = pos < 2
    bufs = {"w": w, "p": p}

    def dev(xx, yy, zz, kk):
        return (zz * 8 + yy * 2 + kk, xx)

    def up(v, n=1):
        return lax.rem(v + n, 4)

    peer = dev(x, y, z, 1 - k)
    sends = []

    def copy(src, dst, ssem, rsem, device):
        return pltpu.make_async_remote_copy(
            src_ref=src, dst_ref=dst, send_sem=ssem, recv_sem=rsem, device_id=device, device_id_type=MESH
        )

    free = list(range(POOL))

    def send(src, dst, rsem, device, cond=None):
        ssem = free.pop(0)

        def go():
            copy(src, dst, pool.at[ssem], rsem, device).start()

        if cond is None:
            go()
        else:
            pl.when(cond)(go)
        sends.append((src, dst, ssem, rsem, device, cond))

    def recv(dst, rsem, cond=None):
        def go():
            copy(dst, dst, pool.at[0], rsem, peer).wait_recv()

        if cond is None:
            go()
        else:
            pl.when(cond)(go)

    def ref_of(stage, color, phase, where, half):
        name, c0, cn, rows = STAGES[stage]
        buf = bufs[name]
        r0, rn, rh = rows[color]
        cols = pl.ds(c0, cn)
        rr = pl.ds(r0, rn)
        parts = {None: rr, 0: pl.ds(r0, rh), 1: pl.ds(r0 + rh, rn - rh)}
        two = {None: slice(None), 0: pl.ds(0, 2), 1: pl.ds(2, 2)}
        one = {None: slice(None), 0: pl.ds(0, 1), 1: pl.ds(1, 1)}
        axis = ORDERS[color][phase]
        if phase == 0:
            if axis == "x":
                return buf.at[where, z, y, parts[half], cols]
            if axis == "y":
                return buf.at[xi0, z, where, parts[half], cols]
            return buf.at[xi0, where, y, parts[half], cols]
        if color == 0:
            if axis == "y":
                return buf.at[one[half], z, where, rr, cols]
            return buf.at[one[half], where, :, rr, cols]
        if color == 1:
            if axis == "z":
                return buf.at[xi0, where, two[half], rr, cols]
            return buf.at[where, two[half], :, rr, cols]
        if axis == "x":
            return buf.at[where, two[half], y, rr, cols]
        return buf.at[one[half], :, where, rr, cols]

    slots = {}

    def first_slot(stage, color):
        return slots[stage, color, 0, 0]

    def context(stage, color, phase):
        axis = ORDERS[color][phase]
        rs = [ag_recv.at[slots.setdefault((stage, color, phase, i), len(slots))] for i in SLOTS[phase > 0, axis == "x"]]
        only_sources = is_source if ORDERS[color].index("x") > phase else None
        return axis, rs, only_sources

    def ring(axis):
        if axis == "y":
            return y, dev(x, up(y), z, k), dev(x, up(y, 3), z, k)
        return z, dev(x, y, up(z), k), dev(x, y, up(z, 3), k)

    def start1(stage, color, phase):
        axis, rs, cond = context(stage, color, phase)
        if axis == "x":
            if phase == 0:
                r = ref_of(stage, color, phase, xi0, None)
                for d in (1, 3, 2):
                    send(r, r, ag_recv.at[first_slot(stage, color) + xi0], dev(up(x, d), y, z, k), is_source)
                return
            inward = dev(jnp.where(pos == 0, up(x), up(x, 3)), y, z, k)
            outward = dev(jnp.where(pos == 0, up(x, 3), up(x)), y, z, k)
            h0, h1 = (ref_of(stage, color, phase, xi0, h) for h in (0, 1))
            send(h0, h0, rs[0], inward, is_source)
            send(h1, h1, rs[0], outward, is_source)
            send(h1, h1, rs[1], inward, is_source)
            send(h0, h0, rs[1], outward, is_source)
        else:
            at, right, left = ring(axis)
            if phase == 0:
                r = ref_of(stage, color, phase, at, None)
                send(r, r, rs[0], right, cond)
                send(r, r, rs[1], left, cond)
                across = dev(x, up(y, 2), z, k) if axis == "y" else dev(x, y, up(z, 2), k)
                send(r, r, rs[2], across, cond)
                return
            h0, h1 = (ref_of(stage, color, phase, at, h) for h in (0, 1))
            send(h0, h0, rs[0], right, cond)
            send(h1, h1, rs[1], left, cond)
            send(h1, h1, rs[2], right, cond)
            send(h0, h0, rs[3], left, cond)

    def turn(stage, color, phase):
        axis, rs, cond = context(stage, color, phase)
        if axis == "x":
            other = 1 - xi0
            h0, h1 = (ref_of(stage, color, phase, other, h) for h in (0, 1))
            to_low = dev(jnp.where(pos == 0, up(x, 3), up(x)), y, z, k)
            to_high = dev(jnp.where(pos == 2, up(x), up(x, 3)), y, z, k)
            recv(h0, rs[0], pos < 2)
            recv(h1, rs[0], pos >= 2)
            send(h0, h0, rs[2], to_low, pos < 2)
            send(h1, h1, rs[3], to_high, pos >= 2)
        else:
            at, right, left = ring(axis)
            h0 = ref_of(stage, color, phase, up(at, 3), 0)
            h1 = ref_of(stage, color, phase, up(at), 1)
            recv(h0, rs[0], cond)
            send(h0, h0, rs[4], right, cond)
            recv(h1, rs[1], cond)
            send(h1, h1, rs[5], left, cond)

    def finish(stage, color, phase):
        axis, rs, cond = context(stage, color, phase)
        if axis == "x":
            other = 1 - xi0
            if phase == 0:
                base = first_slot(stage, color)
                recv(ref_of(stage, color, phase, other, None), ag_recv.at[base + other])
                recv(ref_of(stage, color, phase, xi0, None), ag_recv.at[base + xi0], pos >= 2)
                return
            recv(ref_of(stage, color, phase, other, 1), rs[1], pos < 2)
            recv(ref_of(stage, color, phase, other, 0), rs[1], pos >= 2)
            recv(ref_of(stage, color, phase, xi0, 0), rs[2], pos >= 2)
            recv(ref_of(stage, color, phase, xi0, 1), rs[3], pos >= 2)
        else:
            at, _, _ = ring(axis)
            if phase == 0:
                for d, i in ((3, 0), (1, 1), (2, 2)):
                    recv(ref_of(stage, color, phase, up(at, d), None), rs[i], cond)
                return
            recv(ref_of(stage, color, phase, up(at, 3), 1), rs[2], cond)
            recv(ref_of(stage, color, phase, up(at), 0), rs[3], cond)
            recv(ref_of(stage, color, phase, up(at, 2), 0), rs[4], cond)
            recv(ref_of(stage, color, phase, up(at, 2), 1), rs[5], cond)

    def all_colors(step, stage, phase):
        for color in range(3):
            step(stage, color, phase)

    def flush(count=None):
        for _ in range(len(sends) if count is None else count):
            src, dst, ssem, rsem, device, cond = sends.pop(0)

            def done():
                copy(src, dst, pool.at[ssem], rsem, device).wait_send()

            if cond is None:
                done()
            else:
                pl.when(cond)(done)
            free.append(ssem)

    own_rows = pl.ds(pl.multiple_of(k * 64, 64), 64)
    barrier = pltpu.get_barrier_semaphore()
    y_up, z_up = up(y), up(z)
    partners = [
        peer, dev(up(x), y, z, k), dev(up(x, 3), y, z, k),
        dev(x, y_up, z, k), dev(x, up(y, 3), z, k), dev(x, y, z_up, k), dev(x, y, up(z, 3), k),
        dev(up(x, 2), y, z, k), dev(x, up(y, 2), z, k), dev(x, y, up(z, 2), k),
    ]
    for partner in partners:
        pl.semaphore_signal(barrier, inc=1, device_id=partner, device_id_type=MESH)
    own = pl.multiple_of(x * 256, 256)
    local = pltpu.make_async_copy(tokens.at[pl.ds(own, 256), :], x_buf.at[k, x], loc_sem)
    local.start()
    for load in loads:
        load.wait()
    shard = jnp.concatenate([wcv[...], wcg[...], wq[...], wk[...], wv[...]], axis=1)

    @pl.when(is_source)
    def _():
        w[xi0, z, y, own_rows, :] = shard

    @pl.when(jnp.logical_not(is_source))
    def _():
        mine_w[...] = shard

    mine_p[...] = jnp.concatenate([attn_proj[...], conv_proj[...]], axis=0)
    small[xi0, 0:31, :] = taps[...]
    small[xi0, 31:32, :] = conv_gain[...]
    small[xi0, 32:33, :] = jnp.concatenate(
        [jnp.broadcast_to(sinks[:, h : h + 1], (1, 64)) for h in range(4)], axis=1
    )

    pl.semaphore_wait(barrier, len(partners))

    not_source = jnp.logical_not(is_source)
    slot = w.at[xi0, z, y, own_rows, :]
    send(mine_w, slot, d2d_recv.at[0], peer, not_source)
    send(mine_p, peer_p, d2d_recv.at[1], peer)
    peer_rows = pl.ds(pl.multiple_of((1 - k) * 64, 64), 64)
    recv(w.at[xi0, z, y, peer_rows, :], d2d_recv.at[0], is_source)
    all_colors(start1, 0, 0)
    all_colors(start1, 1, 0)

    right, left, across = dev(up(x), y, z, k), dev(up(x, 3), y, z, k), up(x, 2)

    def token_sends(far):
        for to, device, i in ((up(x), right, 0), (up(x, 3), left, 1)):
            if far:
                block = tokens.at[pl.ds(pl.multiple_of(across * 256 + i * 128, 128), 128), :]
                send(block, hop.at[i], hop_recv.at[i], device)
            else:
                block = tokens.at[pl.ds(pl.multiple_of(to * 256, 256), 256), :]
                send(block, x_buf.at[k, x], tok_recv.at[i], device)

    def token_hops():
        for origin, device, i in ((up(x, 3), right, 0), (up(x), left, 1)):
            recv(hop.at[i], hop_recv.at[i])
            send(hop.at[i], x_buf.at[k, origin, pl.ds(i * 128, 128), :], tok_recv.at[2 + i], device)

    def tokens_on():
        for i, origin in ((0, up(x, 3)), (1, up(x))):
            recv(x_buf.at[k, origin], tok_recv.at[i])
            send(x_buf.at[k, origin], x_buf.at[k, origin], fwd_recv.at[1 + i], peer)
        for i in (0, 1):
            recv(x_buf.at[k, across, pl.ds(i * 128, 128), :], tok_recv.at[2 + i])
        send(x_buf.at[k, across], x_buf.at[k, across], fwd_recv.at[3], peer)

    def small_on():
        recv(small.at[1 - xi0], sm_recv.at[1 - xi0])
        beyond = dev(jnp.where(jnp.logical_or(pos == 0, pos == 3), up(x, 3), up(x)), y, z, k)
        send(small.at[1 - xi0], small.at[1 - xi0], sm_recv.at[1 - xi0], beyond, is_source)

    token_sends(True)
    recv(peer_p, d2d_recv.at[1])

    @pl.when(is_source)
    def _():
        a, b = mine_p[...], peer_p[...]
        low = jnp.where(k == 0, a, b)
        high = jnp.where(k == 0, b, a)
        p[xi0, z, y, 0:256, :] = jnp.concatenate([low[:64], high[:64]], axis=0).T
        p[xi0, z, y, 256:512, :] = jnp.concatenate([low[64:], high[64:]], axis=0).T

    all_colors(start1, 2, 0)
    token_sends(False)
    send(tokens.at[pl.ds(own, 256), :], x_buf.at[k, x], fwd_recv.at[0], peer)
    mine_small = small.at[xi0]
    for i, device in enumerate((right, left)):
        send(mine_small, mine_small, sm_recv.at[xi0], device, is_source)
    all_colors(finish, 0, 0)
    initial = len(sends)
    all_colors(start1, 0, 1)
    all_colors(finish, 1, 0)
    all_colors(start1, 1, 1)
    all_colors(finish, 2, 0)
    token_hops()
    all_colors(turn, 0, 1)
    all_colors(start1, 2, 1)
    all_colors(turn, 1, 1)
    all_colors(finish, 0, 1)
    early = len(sends) - initial
    all_colors(start1, 0, 2)
    all_colors(turn, 2, 1)
    all_colors(finish, 1, 1)
    flush(initial)
    small_on()
    tokens_on()
    all_colors(turn, 0, 2)
    all_colors(start1, 1, 2)
    local.wait()
    recv(x_buf.at[1 - k, x], fwd_recv.at[0])
    for i, origin in ((1, up(x, 3)), (2, up(x)), (3, across)):
        recv(x_buf.at[1 - k, origin], fwd_recv.at[i])

    def norm_rows(i, _):
        s, r = i // 8, lax.rem(i, 8)
        rows = pl.ds(pl.multiple_of(r * 32, 32), 32)
        parts = [x_buf[s, f, rows, :].astype(F32) for f in range(4)]
        square = sum(jnp.sum(v * v, axis=-1, keepdims=True) for v in parts)
        scale = lax.rsqrt(square * (1.0 / 2048) + EPSILON)
        for f in range(4):
            normed[pl.ds(pl.multiple_of(i * 32, 32), 32), f * 512 : f * 512 + 512] = (
                parts[f] * scale * mix_gain[:, f * 512 : f * 512 + 512]
            ).astype(BF)
        return 0

    lax.fori_loop(0, 16, norm_rows, 0)

    flush(early)
    middle = len(sends)
    all_colors(finish, 2, 1)
    all_colors(finish, 0, 2)

    lane = lax.broadcasted_iota(jnp.int32, (256, 128), 1)
    low_lane = lane < 64
    key_row = jnp.concatenate([key_gain[...], jnp.ones_like(key_gain[...])], axis=1)
    query_row = jnp.concatenate([query_gain[...], query_gain[...]], axis=1)

    def project(s, xi, cols):
        lhs = normed[pl.ds(pl.multiple_of(s * 256, 256), 256), :]
        rhs = w[xi, :, :, :, cols[0] : cols[1]].reshape(2048, cols[1] - cols[0])
        return jnp.dot(lhs, rhs, preferred_element_type=F32)

    def gated_part(i, _):
        xi, s = i // 2, lax.rem(i, 2)
        both = project(s, xi, (0, 512))
        value, gate = both[:, :256], both[:, 256:]
        rounded = (value * jax.nn.sigmoid(gate)).astype(BF)
        gated = rounded.astype(F32)
        for half in (0, 1):
            lanes = slice(half * 128, half * 128 + 128)
            ge[s, xi * 2 + half, 16:272, :] = gated[:, lanes]
            edge_send[s, 0, xi * 2 + half] = rounded[240:, lanes]
            edge_send[s, 1, xi * 2 + half] = rounded[:16, lanes]
        return 0

    lax.fori_loop(0, 4, gated_part, 0)

    def neighbour(s, side):
        wraps, over = (x == 3, 1) if side == 0 else (x == 0, 15)
        step = jnp.where(jnp.logical_and(wraps, s == 1 - side), over, 0)
        return (lax.rem(q + step, 16) * 2 + k, up(x, 1 if side == 0 else 3)), jnp.where(wraps, 1 - s, s)

    SIDES = ((0, 0), (0, 1), (1, 0), (1, 1))
    is_first = jnp.logical_and(q == 0, x == 0)
    is_last = jnp.logical_and(q == 15, x == 3)

    for s, side in SIDES:
        to, seg = neighbour(s, side)
        send(edge_send.at[s, side], edge_recv.at[seg, side],
             halo_recv.at[4 + seg * 2 + side], to)
    all_colors(turn, 1, 2)
    all_colors(start1, 2, 2)
    recv(small.at[xi0], sm_recv.at[xi0], not_source)
    for s, side in SIDES:
        recv(edge_recv.at[s, side], halo_recv.at[4 + s * 2 + side])
        ge[s, :, side * 272 : side * 272 + 16, :] = edge_recv[s, side].astype(F32)

    @pl.when(is_first)
    def _():
        ge[0, :, 0:16, :] = jnp.zeros((4, 16, 128), F32)

    @pl.when(is_last)
    def _():
        ge[1, :, 272:288, :] = jnp.zeros((4, 16, 128), F32)

    def conv_block(i, _):
        s, cb = i // 4, lax.rem(i, 4)
        xi, half = cb // 2, lax.rem(cb, 2)
        tap_rows = jnp.where(half == 0, small[xi, :, 0:128], small[xi, :, 128:256])
        for r in (0, 128):
            total = jnp.zeros((128, 128), F32)
            for t in range(31):
                total = total + tap_rows[t : t + 1, :] * ge[s, cb, r + 1 + t : r + 129 + t, :]
            conv[cb, pl.ds(pl.multiple_of(s * 256, 256) + r, 128), :] = total
        return 0

    lax.fori_loop(0, 8, conv_block, 0)

    all_colors(finish, 1, 2)

    def project_both(s, cols):
        lhs = normed[pl.ds(pl.multiple_of(s * 256, 256), 256), :]
        width = cols[1] - cols[0]
        rhs = jnp.concatenate([w[xi, :, :, :, cols[0] : cols[1]].reshape(2048, width) for xi in (0, 1)], axis=1)
        both = jnp.dot(lhs, rhs, preferred_element_type=F32)
        return both[:, :width], both[:, width:]

    def first_part(s, _):
        for xi, kv in enumerate(project_both(s, KV)):
            square = jnp.sum(jnp.where(low_lane, kv * kv, 0.0), axis=-1, keepdims=True)
            keyed = kv * lax.rsqrt(square * (1.0 / 64) + EPSILON) * key_row
            kve[s, xi, 128:384, :] = jnp.where(low_lane, keyed, kv).astype(BF)
        return 0

    lax.fori_loop(0, 2, first_part, 0)
    for s, side in SIDES:
        to, seg = neighbour(s, side)
        src, dst = (256, 0) if side == 0 else (128, 384)
        send(kve.at[s, :, pl.ds(src, 128), :], kve.at[seg, :, pl.ds(dst, 128), :], halo_recv.at[seg * 2 + side], to)
    def stats(i, _):
        rows = pl.ds(pl.multiple_of(i * 64, 64), 64)
        blocks = [conv[cb, rows, :] for cb in range(4)]
        mean = jnp.sum(blocks[0] + blocks[1] + blocks[2] + blocks[3], axis=-1, keepdims=True) * (1.0 / 512)
        dev_sq = sum((b - mean) * (b - mean) for b in blocks)
        m2 = jnp.sum(dev_sq, axis=-1, keepdims=True)
        stat_own[rows, :] = jnp.where(low_lane[:64], mean, m2)
        return 0

    lax.fori_loop(0, 8, stats, 0)
    send(stat_own, stat_peer, stat_recv.at[0], peer)

    def query_part(s, _):
        for xi, full in enumerate(project_both(s, Q)):
            for pair in (0, 1):
                v = full[:, pair * 128 : pair * 128 + 128]
                sq = v * v
                even = jnp.sum(jnp.where(low_lane, sq, 0.0), axis=-1, keepdims=True)
                odd = jnp.sum(jnp.where(low_lane, 0.0, sq), axis=-1, keepdims=True)
                scale = lax.rsqrt(jnp.where(low_lane, even, odd) * (1.0 / 64) + EPSILON)
                rounded = (v * scale * query_row).astype(BF).astype(F32) * 0.125
                qn[xi * 2 + pair, pl.ds(pl.multiple_of(s * 256, 256), 256), :] = rounded.astype(BF)
        return 0

    lax.fori_loop(0, 2, query_part, 0)
    recv(stat_peer, stat_recv.at[0])

    def feature(i, _):
        rows = pl.ds(pl.multiple_of(i * 64, 64), 64)
        a, b = stat_own[rows, :], stat_peer[rows, :]
        mean = 0.5 * (a[:, 0:1] + b[:, 0:1])
        gap = a[:, 0:1] - b[:, 0:1]
        spread = (a[:, 64:65] + b[:, 64:65] + gap * gap * 256.0) * (1.0 / 1024)
        scale = lax.rsqrt(spread + EPSILON)
        for cb in range(4):
            xi, half = cb // 2, cb % 2
            gain = small[xi, 31:32, half * 128 : half * 128 + 128]
            v = (conv[cb, rows, :] - mean) * scale * gain
            feats[rows, xi * 512 + 256 + half * 128 : xi * 512 + 384 + half * 128] = (v * jax.nn.sigmoid(v)).astype(BF)
        return 0

    lax.fori_loop(0, 8, feature, 0)
    all_colors(turn, 2, 2)
    flush(middle)
    row_i = lax.rem(lax.broadcasted_iota(jnp.int32, (256, 384), 0), 128)
    col_i = lax.broadcasted_iota(jnp.int32, (256, 384), 1)
    lane384 = lax.broadcasted_iota(jnp.int32, (384, 128), 1) < 64

    def attention(i):
        s, b = i // 2, i % 2
        base = s * 256 + b * 128
        first = jnp.where(jnp.logical_and(is_first, s == 0), 128, 0) - b * 128
        end = jnp.where(jnp.logical_and(is_last, s == 1), 384, 512) - b * 128
        reach = col_i - row_i
        allowed = (reach >= 0) & (reach <= 256) & (col_i >= first) & (col_i < end)
        nt = (((1,), (1,)), ((), ()))

        def mix(heads, keys, values):
            scores = lax.dot_general(heads, keys.astype(BF), nt, preferred_element_type=F32)
            weights = jnp.where(allowed, jnp.exp(scores), 0.0).astype(BF)
            return jnp.dot(weights, values.astype(BF), preferred_element_type=F32)

        for xi in (0, 1):
            kv = kve[s, xi, b * 128 : b * 128 + 384, :].astype(F32)
            swapped = pltpu.roll(kv, 64, 1)
            both = jnp.concatenate([qn[xi * 2 + pair, pl.ds(base, 128), :] for pair in (0, 1)], axis=0).astype(F32)
            even = jnp.where(low_lane, both, 0.0).astype(BF)
            odd = jnp.where(low_lane, 0.0, both).astype(BF)
            o_even = mix(even, kv, jnp.where(lane384, swapped, 1.0))
            o_odd = mix(odd, swapped, jnp.where(lane384, 1.0, kv))
            number = jnp.where(low_lane, o_even, o_odd)
            weight = pltpu.roll(jnp.where(low_lane, o_odd, o_even), 64, 1)
            sink = jnp.exp(small[xi, 32:33, :])
            for pair in (0, 1):
                rows, lanes = slice(pair * 128, pair * 128 + 128), slice(pair * 128, pair * 128 + 128)
                col = xi * 512 + pair * 128
                feats[pl.ds(base, 128), col : col + 128] = (number[rows] / (weight[rows] + sink[:, lanes])).astype(BF)

    for s, b in SIDES:
        recv(kve.at[s, :, pl.ds(b * 384, 128), :], halo_recv.at[s * 2 + b])
        attention(s * 2 + b)

    all_colors(finish, 2, 2)

    for nb in range(4):
        rhs = jnp.concatenate(
            [jnp.concatenate([p[xi, nb, yy] for yy in range(4)], axis=1) for xi in (0, 1)], axis=0
        )
        part = jnp.dot(feats[...], rhs, preferred_element_type=F32).reshape(2, 256, 512)
        part_send[nb] = part.astype(BF)
        send(part_send.at[nb, 1 - k], part_recv.at[nb], out_recv.at[nb], peer)
        part_own[nb] = part
    for nb in range(4):
        recv(part_recv.at[nb], out_recv.at[nb])
        out[:, nb * 512 : nb * 512 + 512] = (part_own[nb, k] + part_recv[nb].astype(F32)).astype(BF)
    flush()


def on_device(tokens, mix_gain, wq, wk, wv, wcv, wcg, query_gain, key_gain, sinks, taps, conv_gain, attn_proj, conv_proj):
    vmem = pl.BlockSpec(memory_space=pltpu.VMEM)
    dma = pltpu.SemaphoreType.DMA
    arrays = (
        tokens, mix_gain.reshape(1, -1), wq, wk, wv, wcv, wcg, query_gain.reshape(1, -1), key_gain.reshape(1, -1),
        sinks.reshape(1, -1), taps, conv_gain.reshape(1, -1), attn_proj.T, conv_proj.T,
    )
    return pl.pallas_call(
        kernel,
        out_shape=jax.ShapeDtypeStruct((256, 2048), BF),
        in_specs=[pl.BlockSpec(memory_space=pltpu.HBM)] * 14,
        out_specs=vmem,
        scratch_shapes=[
            *(pltpu.VMEM(a.shape, a.dtype) for a in arrays[1:]),
            pltpu.VMEM((2, 4, 4, 128, 896), BF),
            pltpu.VMEM((2, 4, 4, 512, 128), BF),
            pltpu.VMEM((64, 896), BF),
            pltpu.VMEM((128, 256), BF),
            pltpu.VMEM((128, 256), BF),
            pltpu.VMEM((2, 40, 256), F32),
            pltpu.VMEM((2, 128, 512), BF),
            pltpu.VMEM((2, 2, 4, 16, 128), BF),
            pltpu.VMEM((2, 2, 4, 16, 128), BF),
            pltpu.VMEM((2, 4, 256, 512), BF),
            pltpu.VMEM((512, 2048), BF),
            pltpu.VMEM((4, 512, 128), BF),
            pltpu.VMEM((2, 2, 512, 128), BF),
            pltpu.VMEM((2, 4, 288, 128), F32),
            pltpu.VMEM((4, 512, 128), F32),
            pltpu.VMEM((512, 128), F32),
            pltpu.VMEM((512, 128), F32),
            pltpu.VMEM((512, 1024), BF),
            pltpu.VMEM((4, 2, 256, 512), F32),
            pltpu.VMEM((4, 2, 256, 512), BF),
            pltpu.VMEM((4, 256, 512), BF),
            dma((13,)), dma((POOL,)), dma((SLOT_COUNT,)), dma((2,)), dma((4,)), dma((2,)), dma((4,)), dma(()), dma((2,)),
            dma((8,)), dma((1,)), dma((4,)),
        ],
        compiler_params=pltpu.CompilerParams(
            collective_id=0, has_side_effects=True, vmem_limit_bytes=44 * 1024 * 1024
        ),
        name="layer",
    )(*(pltpu.with_memory_space_constraint(a, pltpu.HBM) for a in arrays))


def solution(mesh):
    placed = (
        P("sp", "tp"), P(), P("sp", "tp"), P("sp", "tp"), P("sp", "tp"), P("sp", "tp"), P("sp", "tp"),
        P(), P(), P("tp"), P(None, "tp"), P("tp"), P("tp", "sp"), P("tp", "sp"),
    )
    return jax.shard_map(
        on_device, mesh=mesh, in_specs=placed, out_specs=P(("sp", "tp"), None), check_vma=False
    )
```

time: 88.7 us -> 75.6 us (0.85)
  Pallas kernels: 86.2 us -> 74.5 us
  local copies, waits for them, and re-layouts: 2.3 us -> 0.97 us
    pallas_call x1, Pallas kernels: 86.2 us -> 74.5 us  [on_device(): pl.pallas_call(kernel, out_shape=jax.ShapeDtypeStruct((256, 2048), BF), i...]
    unnamed x1, local copies, waits for them, and re-layouts: 2.3 us -> 0.97 us
where the time goes in v4:
time: 75.6 us; the launch traced here: 75.5 us
  Pallas kernels  74.5 us (99%)
  local copies, waits for them, and re-layouts  0.97 us (1%)
    pallas_call x1, Pallas kernels, on_device(): pl.pallas_call(kernel, out_shape=jax.ShapeDtypeStruct((256, 2048), BF), i...  74.5 us

profile of v4, /device:TPU:1, one launch (start us, length us, event | category | flops | bytes accessed | tf_op | source)
XLA Modules:
  0.0 75.5 jit_solution(3801176695570392283)
XLA Ops:
  0.0 74.5 %layer.1 = bf16[256,2048]{1,0:T(8,128)(2,1)S(1)} custom-call(bf16[1024,512]{1,0:T(8,128)(2,1)} %tokens.1, f32[1,2048]{1,0:T(1,128)} %bitcast.9, bf16[64,256]{1,0:T(8,128)(2,1)} %rest_1_.1, bf16[64,64]{1,0:T(8,128)(2,1)} %rest_2_.1, bf16[64,64]{1,0:T(8,128)(2,1)} %rest_3_.1, bf16[64,256]{1,0:T(8,128)(2,1)} %rest_4_.1, bf16[64,256]{1,0:T(8,128)(2,1)} %rest_5_.1, ...), custom_call_target="tpu_custom_call" | custom-call | tf_op jit(solution)/shard_map/layer/pallas_call | solution.py:547
  74.5 1.0 %copy.16 = bf16[256,2048]{1,0:T(8,128)(2,1)} copy(bf16[256,2048]{1,0:T(8,128)(2,1)S(1)} %layer.1) | data formatting | bytes 2097152

commit v5 on v4

--- a/solution.py
+++ b/solution.py
@@ -12,9 +12,9 @@
 
 CV, CG, Q, KV = (0, 256), (256, 512), (512, 768), (768, 896)
 STAGES = (
-    ("w", 0, 512, ((0, 48, 32), (48, 32, 16), (80, 48, 32))),
-    ("w", 512, 384, ((0, 48, 32), (48, 32, 16), (80, 48, 32))),
-    ("p", 0, 128, ((0, 176, 96), (176, 160, 80), (336, 176, 96))),
+    ("w", 0, 512, ((0, 64, 32), (64, 16, 16), (80, 48, 32))),
+    ("w", 512, 384, ((0, 48, 32), (48, 16, 16), (64, 64, 32))),
+    ("p", 0, 128, ((0, 160, 80), (160, 192, 96), (352, 160, 80))),
 )
 ORDERS = ("xyz", "yzx", "zxy")
 SLOTS = {(False, True): range(2), (False, False): range(3), (True, True): range(4), (True, False): range(6)}
@@ -90,16 +90,15 @@
         r0, rn, rh = rows[color]
         cols = pl.ds(c0, cn)
         rr = pl.ds(r0, rn)
-        parts = {None: rr, 0: pl.ds(r0, rh), 1: pl.ds(r0 + rh, rn - rh)}
         two = {None: slice(None), 0: pl.ds(0, 2), 1: pl.ds(2, 2)}
         one = {None: slice(None), 0: pl.ds(0, 1), 1: pl.ds(1, 1)}
         axis = ORDERS[color][phase]
         if phase == 0:
             if axis == "x":
-                return buf.at[where, z, y, parts[half], cols]
+                return buf.at[where, z, y, rr, cols]
             if axis == "y":
-                return buf.at[xi0, z, where, parts[half], cols]
-            return buf.at[xi0, where, y, parts[half], cols]
+                return buf.at[xi0, z, where, rr, cols]
+            return buf.at[xi0, where, y, rr, cols]
         if color == 0:
             if axis == "y":
                 return buf.at[one[half], z, where, rr, cols]
@@ -278,10 +277,12 @@
             recv(hop.at[i], hop_recv.at[i])
             send(hop.at[i], x_buf.at[k, origin, pl.ds(i * 128, 128), :], tok_recv.at[2 + i], device)
 
-    def tokens_on():
+    def tokens_near():
         for i, origin in ((0, up(x, 3)), (1, up(x))):
             recv(x_buf.at[k, origin], tok_recv.at[i])
             send(x_buf.at[k, origin], x_buf.at[k, origin], fwd_recv.at[1 + i], peer)
+
+    def tokens_far():
         for i in (0, 1):
             recv(x_buf.at[k, across, pl.ds(i * 128, 128), :], tok_recv.at[2 + i])
         send(x_buf.at[k, across], x_buf.at[k, across], fwd_recv.at[3], peer)
@@ -291,7 +292,6 @@
         beyond = dev(jnp.where(jnp.logical_or(pos == 0, pos == 3), up(x, 3), up(x)), y, z, k)
         send(small.at[1 - xi0], small.at[1 - xi0], sm_recv.at[1 - xi0], beyond, is_source)
 
-    token_sends(True)
     recv(peer_p, d2d_recv.at[1])
 
     @pl.when(is_source)
@@ -302,51 +302,59 @@
         p[xi0, z, y, 0:256, :] = jnp.concatenate([low[:64], high[:64]], axis=0).T
         p[xi0, z, y, 256:512, :] = jnp.concatenate([low[64:], high[64:]], axis=0).T
 
+    def onward(last, following):
+        for color in range(3):
+            finish(last[0], color, last[1])
+            start1(following[0], color, following[1])
+
     all_colors(start1, 2, 0)
+    onward((0, 0), (0, 1))
+    onward((1, 0), (1, 1))
+    token_sends(True)
+    all_colors(finish, 2, 0)
+    initial = len(sends)
+    all_colors(turn, 0, 1)
+    all_colors(start1, 2, 1)
+    all_colors(turn, 1, 1)
     token_sends(False)
     send(tokens.at[pl.ds(own, 256), :], x_buf.at[k, x], fwd_recv.at[0], peer)
     mine_small = small.at[xi0]
-    for i, device in enumerate((right, left)):
+    for device in (right, left):
         send(mine_small, mine_small, sm_recv.at[xi0], device, is_source)
-    all_colors(finish, 0, 0)
-    initial = len(sends)
-    all_colors(start1, 0, 1)
-    all_colors(finish, 1, 0)
-    all_colors(start1, 1, 1)
-    all_colors(finish, 2, 0)
+    onward((0, 1), (0, 2))
+    early = len(sends) - initial
     token_hops()
-    all_colors(turn, 0, 1)
-    all_colors(start1, 2, 1)
-    all_colors(turn, 1, 1)
-    all_colors(finish, 0, 1)
-    early = len(sends) - initial
-    all_colors(start1, 0, 2)
+    flush(initial)
     all_colors(turn, 2, 1)
-    all_colors(finish, 1, 1)
-    flush(initial)
+    for color in (0, 2, 1):
+        turn(0, color, 2)
+        finish(1, color, 1)
+        start1(1, color, 2)
+        if color == 2:
+            tokens_near()
+    tokens_far()
     small_on()
-    tokens_on()
-    all_colors(turn, 0, 2)
-    all_colors(start1, 1, 2)
     local.wait()
+
+    def norm_rows(s):
+        def body(r, _):
+            rows = pl.ds(pl.multiple_of(r * 32, 32), 32)
+            parts = [x_buf[s, f, rows, :].astype(F32) for f in range(4)]
+            square = sum(jnp.sum(v * v, axis=-1, keepdims=True) for v in parts)
+            scale = lax.rsqrt(square * (1.0 / 2048) + EPSILON)
+            for f in range(4):
+                normed[pl.ds(pl.multiple_of(s * 256 + r * 32, 32), 32), f * 512 : f * 512 + 512] = (
+                    parts[f] * scale * mix_gain[:, f * 512 : f * 512 + 512]
+                ).astype(BF)
+            return 0
+
+        lax.fori_loop(0, 8, body, 0)
+
+    norm_rows(k)
     recv(x_buf.at[1 - k, x], fwd_recv.at[0])
     for i, origin in ((1, up(x, 3)), (2, up(x)), (3, across)):
         recv(x_buf.at[1 - k, origin], fwd_recv.at[i])
-
-    def norm_rows(i, _):
-        s, r = i // 8, lax.rem(i, 8)
-        rows = pl.ds(pl.multiple_of(r * 32, 32), 32)
-        parts = [x_buf[s, f, rows, :].astype(F32) for f in range(4)]
-        square = sum(jnp.sum(v * v, axis=-1, keepdims=True) for v in parts)
-        scale = lax.rsqrt(square * (1.0 / 2048) + EPSILON)
-        for f in range(4):
-            normed[pl.ds(pl.multiple_of(i * 32, 32), 32), f * 512 : f * 512 + 512] = (
-                parts[f] * scale * mix_gain[:, f * 512 : f * 512 + 512]
-            ).astype(BF)
-        return 0
-
-    lax.fori_loop(0, 16, norm_rows, 0)
-
+    norm_rows(1 - k)
     flush(early)
     middle = len(sends)
     all_colors(finish, 2, 1)
@@ -358,12 +366,11 @@
     query_row = jnp.concatenate([query_gain[...], query_gain[...]], axis=1)
 
     def project(s, xi, cols):
-        lhs = normed[pl.ds(pl.multiple_of(s * 256, 256), 256), :]
+        lhs = normed[pl.ds(s * 256, 256), :]
         rhs = w[xi, :, :, :, cols[0] : cols[1]].reshape(2048, cols[1] - cols[0])
         return jnp.dot(lhs, rhs, preferred_element_type=F32)
 
-    def gated_part(i, _):
-        xi, s = i // 2, lax.rem(i, 2)
+    def gated_part(s, xi):
         both = project(s, xi, (0, 512))
         value, gate = both[:, :256], both[:, 256:]
         rounded = (value * jax.nn.sigmoid(gate)).astype(BF)
@@ -373,9 +380,6 @@
             ge[s, xi * 2 + half, 16:272, :] = gated[:, lanes]
             edge_send[s, 0, xi * 2 + half] = rounded[240:, lanes]
             edge_send[s, 1, xi * 2 + half] = rounded[:16, lanes]
-        return 0
-
-    lax.fori_loop(0, 4, gated_part, 0)
 
     def neighbour(s, side):
         wraps, over = (x == 3, 1) if side == 0 else (x == 0, 15)
@@ -386,42 +390,43 @@
     is_first = jnp.logical_and(q == 0, x == 0)
     is_last = jnp.logical_and(q == 15, x == 3)
 
-    for s, side in SIDES:
-        to, seg = neighbour(s, side)
-        send(edge_send.at[s, side], edge_recv.at[seg, side],
-             halo_recv.at[4 + seg * 2 + side], to)
+    for s in (0, 1):
+        for xi in (0, 1):
+            gated_part(s, xi)
+        for side in (0, 1):
+            to, seg = neighbour(s, side)
+            send(edge_send.at[s, side], edge_recv.at[seg, side], halo_recv.at[4 + seg * 2 + side], to)
     all_colors(turn, 1, 2)
     all_colors(start1, 2, 2)
     recv(small.at[xi0], sm_recv.at[xi0], not_source)
-    for s, side in SIDES:
-        recv(edge_recv.at[s, side], halo_recv.at[4 + s * 2 + side])
-        ge[s, :, side * 272 : side * 272 + 16, :] = edge_recv[s, side].astype(F32)
-
-    @pl.when(is_first)
-    def _():
-        ge[0, :, 0:16, :] = jnp.zeros((4, 16, 128), F32)
-
-    @pl.when(is_last)
-    def _():
-        ge[1, :, 272:288, :] = jnp.zeros((4, 16, 128), F32)
-
-    def conv_block(i, _):
-        s, cb = i // 4, lax.rem(i, 4)
+    def conv_block(segment, cb):
         xi, half = cb // 2, lax.rem(cb, 2)
         tap_rows = jnp.where(half == 0, small[xi, :, 0:128], small[xi, :, 128:256])
         for r in (0, 128):
             total = jnp.zeros((128, 128), F32)
             for t in range(31):
-                total = total + tap_rows[t : t + 1, :] * ge[s, cb, r + 1 + t : r + 129 + t, :]
-            conv[cb, pl.ds(pl.multiple_of(s * 256, 256) + r, 128), :] = total
-        return 0
-
-    lax.fori_loop(0, 8, conv_block, 0)
+                total = total + tap_rows[t : t + 1, :] * ge[segment, cb, r + 1 + t : r + 129 + t, :]
+            conv[cb, segment * 256 + r : segment * 256 + r + 128, :] = total
+
+    for s in (0, 1):
+        for side in (0, 1):
+            recv(edge_recv.at[s, side], halo_recv.at[4 + s * 2 + side])
+            ge[s, :, side * 272 : side * 272 + 16, :] = edge_recv[s, side].astype(F32)
+
+        @pl.when(is_first if s == 0 else is_last)
+        def _():
+            ge[s, :, s * 272 : s * 272 + 16, :] = jnp.zeros((4, 16, 128), F32)
+
+        def conv_step(cb, _, s=s):
+            conv_block(s, cb)
+            return 0
+
+        lax.fori_loop(0, 4, conv_step, 0)
 
     all_colors(finish, 1, 2)
 
     def project_both(s, cols):
-        lhs = normed[pl.ds(pl.multiple_of(s * 256, 256), 256), :]
+        lhs = normed[pl.ds(s * 256, 256), :]
         width = cols[1] - cols[0]
         rhs = jnp.concatenate([w[xi, :, :, :, cols[0] : cols[1]].reshape(2048, width) for xi in (0, 1)], axis=1)
         both = jnp.dot(lhs, rhs, preferred_element_type=F32)
@@ -434,8 +439,9 @@
             kve[s, xi, 128:384, :] = jnp.where(low_lane, keyed, kv).astype(BF)
         return 0
 
-    lax.fori_loop(0, 2, first_part, 0)
     for s, side in SIDES:
+        if side == 0:
+            first_part(s, 0)
         to, seg = neighbour(s, side)
         src, dst = (256, 0) if side == 0 else (128, 384)
         send(kve.at[s, :, pl.ds(src, 128), :], kve.at[seg, :, pl.ds(dst, 128), :], halo_recv.at[seg * 2 + side], to)
@@ -460,10 +466,14 @@
                 odd = jnp.sum(jnp.where(low_lane, 0.0, sq), axis=-1, keepdims=True)
                 scale = lax.rsqrt(jnp.where(low_lane, even, odd) * (1.0 / 64) + EPSILON)
                 rounded = (v * scale * query_row).astype(BF).astype(F32) * 0.125
-                qn[xi * 2 + pair, pl.ds(pl.multiple_of(s * 256, 256), 256), :] = rounded.astype(BF)
+                qn[xi * 2 + pair, pl.ds(s * 256, 256), :] = rounded.astype(BF)
         return 0
 
-    lax.fori_loop(0, 2, query_part, 0)
+    for s in (0, 1):
+        query_part(s, 0)
+    late = len(sends) - middle
+    for color in (0, 2, 1):
+        turn(2, color, 2)
     recv(stat_peer, stat_recv.at[0])
 
     def feature(i, _):
@@ -481,7 +491,6 @@
         return 0
 
     lax.fori_loop(0, 8, feature, 0)
-    all_colors(turn, 2, 2)
     flush(middle)
     row_i = lax.rem(lax.broadcasted_iota(jnp.int32, (256, 384), 0), 128)
     col_i = lax.broadcasted_iota(jnp.int32, (256, 384), 1)
@@ -521,6 +530,7 @@
         recv(kve.at[s, :, pl.ds(b * 384, 128), :], halo_recv.at[s * 2 + b])
         attention(s * 2 + b)
 
+    flush(late)
     all_colors(finish, 2, 2)
 
     for nb in range(4):

time: 75.6 us -> 72.6 us (0.960)
  Pallas kernels: 74.5 us -> 71.5 us
    pallas_call x1, Pallas kernels: 74.5 us -> 71.5 us  [on_device(): pl.pallas_call(kernel, out_shape=jax.ShapeDtypeStruct((256, 2048), BF), i...]
where the time goes in v5:
time: 72.6 us; the launch traced here: 72.5 us
  Pallas kernels  71.5 us (98%)
  local copies, waits for them, and re-layouts  0.97 us (1%)
    pallas_call x1, Pallas kernels, on_device(): pl.pallas_call(kernel, out_shape=jax.ShapeDtypeStruct((256, 2048), BF), i...  71.5 us

profile of v5, /device:TPU:1, one launch (start us, length us, event | category | flops | bytes accessed | tf_op | source)
XLA Modules:
  0.0 72.5 jit_solution(3907333198708264303)
XLA Ops:
  0.0 71.5 %layer.1 = bf16[256,2048]{1,0:T(8,128)(2,1)S(1)} custom-call(bf16[1024,512]{1,0:T(8,128)(2,1)} %tokens.1, f32[1,2048]{1,0:T(1,128)} %bitcast.9, bf16[64,256]{1,0:T(8,128)(2,1)} %rest_1_.1, bf16[64,64]{1,0:T(8,128)(2,1)} %rest_2_.1, bf16[64,64]{1,0:T(8,128)(2,1)} %rest_3_.1, bf16[64,256]{1,0:T(8,128)(2,1)} %rest_4_.1, bf16[64,256]{1,0:T(8,128)(2,1)} %rest_5_.1, ...), custom_call_target="tpu_custom_call" | custom-call | tf_op jit(solution)/shard_map/layer/pallas_call | solution.py:557
  71.5 1.0 %copy.16 = bf16[256,2048]{1,0:T(8,128)(2,1)} copy(bf16[256,2048]{1,0:T(8,128)(2,1)S(1)} %layer.1) | data formatting | bytes 2097152

commit v6 on v5

--- a/solution.py
+++ b/solution.py
@@ -399,15 +399,21 @@
     all_colors(turn, 1, 2)
     all_colors(start1, 2, 2)
     recv(small.at[xi0], sm_recv.at[xi0], not_source)
-    def conv_block(segment, cb):
+    def conv_block(segment, cb, chunks):
         xi, half = cb // 2, lax.rem(cb, 2)
         tap_rows = jnp.where(half == 0, small[xi, :, 0:128], small[xi, :, 128:256])
-        for r in (0, 128):
-            total = jnp.zeros((128, 128), F32)
+        for r, n in chunks:
+            total = jnp.zeros((n, 128), F32)
             for t in range(31):
-                total = total + tap_rows[t : t + 1, :] * ge[segment, cb, r + 1 + t : r + 129 + t, :]
-            conv[cb, segment * 256 + r : segment * 256 + r + 128, :] = total
-
+                total = total + tap_rows[t : t + 1, :] * ge[segment, cb, r + 1 + t : r + 1 + n + t, :]
+            conv[cb, segment * 256 + r : segment * 256 + r + n, :] = total
+
+    for s in (0, 1):
+        def inner_step(cb, _, s=s):
+            conv_block(s, cb, ((16, 112), (128, 112)))
+            return 0
+
+        lax.fori_loop(0, 4, inner_step, 0)
     for s in (0, 1):
         for side in (0, 1):
             recv(edge_recv.at[s, side], halo_recv.at[4 + s * 2 + side])
@@ -417,34 +423,11 @@
         def _():
             ge[s, :, s * 272 : s * 272 + 16, :] = jnp.zeros((4, 16, 128), F32)
 
-        def conv_step(cb, _, s=s):
-            conv_block(s, cb)
+        def outer_step(cb, _, s=s):
+            conv_block(s, cb, ((0, 16), (240, 16)))
             return 0
 
-        lax.fori_loop(0, 4, conv_step, 0)
-
-    all_colors(finish, 1, 2)
-
-    def project_both(s, cols):
-        lhs = normed[pl.ds(s * 256, 256), :]
-        width = cols[1] - cols[0]
-        rhs = jnp.concatenate([w[xi, :, :, :, cols[0] : cols[1]].reshape(2048, width) for xi in (0, 1)], axis=1)
-        both = jnp.dot(lhs, rhs, preferred_element_type=F32)
-        return both[:, :width], both[:, width:]
-
-    def first_part(s, _):
-        for xi, kv in enumerate(project_both(s, KV)):
-            square = jnp.sum(jnp.where(low_lane, kv * kv, 0.0), axis=-1, keepdims=True)
-            keyed = kv * lax.rsqrt(square * (1.0 / 64) + EPSILON) * key_row
-            kve[s, xi, 128:384, :] = jnp.where(low_lane, keyed, kv).astype(BF)
-        return 0
-
-    for s, side in SIDES:
-        if side == 0:
-            first_part(s, 0)
-        to, seg = neighbour(s, side)
-        src, dst = (256, 0) if side == 0 else (128, 384)
-        send(kve.at[s, :, pl.ds(src, 128), :], kve.at[seg, :, pl.ds(dst, 128), :], halo_recv.at[seg * 2 + side], to)
+        lax.fori_loop(0, 4, outer_step, 0)
     def stats(i, _):
         rows = pl.ds(pl.multiple_of(i * 64, 64), 64)
         blocks = [conv[cb, rows, :] for cb in range(4)]
@@ -457,6 +440,28 @@
     lax.fori_loop(0, 8, stats, 0)
     send(stat_own, stat_peer, stat_recv.at[0], peer)
 
+    all_colors(finish, 1, 2)
+
+    def project_both(s, cols):
+        lhs = normed[pl.ds(s * 256, 256), :]
+        width = cols[1] - cols[0]
+        rhs = jnp.concatenate([w[xi, :, :, :, cols[0] : cols[1]].reshape(2048, width) for xi in (0, 1)], axis=1)
+        both = jnp.dot(lhs, rhs, preferred_element_type=F32)
+        return both[:, :width], both[:, width:]
+
+    def first_part(s, _):
+        for xi, kv in enumerate(project_both(s, KV)):
+            square = jnp.sum(jnp.where(low_lane, kv * kv, 0.0), axis=-1, keepdims=True)
+            keyed = kv * lax.rsqrt(square * (1.0 / 64) + EPSILON) * key_row
+            kve[s, xi, 128:384, :] = jnp.where(low_lane, keyed, kv).astype(BF)
+        return 0
+
+    for s, side in SIDES:
+        if side == 0:
+            first_part(s, 0)
+        to, seg = neighbour(s, side)
+        src, dst = (256, 0) if side == 0 else (128, 384)
+        send(kve.at[s, :, pl.ds(src, 128), :], kve.at[seg, :, pl.ds(dst, 128), :], halo_recv.at[seg * 2 + side], to)
     def query_part(s, _):
         for xi, full in enumerate(project_both(s, Q)):
             for pair in (0, 1):

time: 72.6 us -> 72.6 us (level)
  no operation moved by 1% of the time
where the time goes in v6:
time: 72.6 us; the launch traced here: 72.5 us
  Pallas kernels  71.5 us (98%)
  local copies, waits for them, and re-layouts  0.97 us (1%)
    pallas_call x1, Pallas kernels, on_device(): pl.pallas_call(kernel, out_shape=jax.ShapeDtypeStruct((256, 2048), BF), i...  71.5 us

profile of v6, /device:TPU:1, one launch (start us, length us, event | category | flops | bytes accessed | tf_op | source)
XLA Modules:
  0.0 72.5 jit_solution(12337776563037746512)
XLA Ops:
  0.0 71.5 %layer.1 = bf16[256,2048]{1,0:T(8,128)(2,1)S(1)} custom-call(bf16[1024,512]{1,0:T(8,128)(2,1)} %tokens.1, f32[1,2048]{1,0:T(1,128)} %bitcast.9, bf16[64,256]{1,0:T(8,128)(2,1)} %rest_1_.1, bf16[64,64]{1,0:T(8,128)(2,1)} %rest_2_.1, bf16[64,64]{1,0:T(8,128)(2,1)} %rest_3_.1, bf16[64,256]{1,0:T(8,128)(2,1)} %rest_4_.1, bf16[64,256]{1,0:T(8,128)(2,1)} %rest_5_.1, ...), custom_call_target="tpu_custom_call" | custom-call | tf_op jit(solution)/shard_map/layer/pallas_call | solution.py:562
  71.5 1.0 %copy.16 = bf16[256,2048]{1,0:T(8,128)(2,1)} copy(bf16[256,2048]{1,0:T(8,128)(2,1)S(1)} %layer.1) | data formatting | bytes 2097152
